TPU v7x, 32 devices: a whole 2x2x4 slice. The times are simulated.
32 devices in a mesh: sp: 8 (over z, core), tp: 4 (over y, x).
Axes of the slice: x: 2, y: 2, z: 4, core: 2. Of those that a mesh axis runs over, the one named last changes fastest.
Arguments:
- stream: bfloat16 [3072, 2048], P('sp'), may hold values from -6 to 6
- inner_act: bfloat16 [3072, 4096], P('sp', 'tp'), may hold values from -6 to 6
- gate_act: bfloat16 [3072, 4096], P('sp', 'tp'), may hold values from -6 to 6
- state_write: bfloat16 [3072, 16, 128], P('sp', 'tp'), may hold values from -6 to 6
- state_read: bfloat16 [3072, 16, 128], P('sp', 'tp'), may hold values from -6 to 6
- step_raw: bfloat16 [3072, 64], P('sp', 'tp'), may hold values from -4.6 to 4.1
- conv_inner: bfloat16 [4, 4096], P(None, 'tp'), may hold values from -3 to 3
- conv_write: bfloat16 [4, 16, 128], P(None, 'tp'), may hold values from -3 to 3
- conv_read: bfloat16 [4, 16, 128], P(None, 'tp'), may hold values from -3 to 3
- step_bias: float32 [64], P('tp'), may hold values from -0.5 to 0.5
- decay_log: float32 [64], P('tp'), may hold values from -13 to -2.52, as said below
- inner_gain: float32 [4096], P('tp'), may hold values from 0.1 to 1.9
- out_weight: bfloat16 [4096, 2048], P('tp'), may hold values from -0.09375 to 0.09375
- ffn_gain: float32 [2048], replicated, may hold values from 0.1 to 1.9
- expert_ids: int32 [3072, 2], P('sp'), may hold values from 0 to 31, all different within a row; in each aligned block of 384 rows (0 to 383, 384 to 767, ...) at most 48 rows name the same one
- expert_weights: float32 [3072, 2], P('sp'), may hold values from 0.1 to 1
- expert_gate: bfloat16 [32, 2048, 1024], P('sp', None, 'tp'), may hold values from -0.125 to 0.125
- expert_up: bfloat16 [32, 2048, 1024], P('sp', None, 'tp'), may hold values from -0.125 to 0.125
- expert_down: bfloat16 [32, 1024, 2048], P('sp', None, 'tp'), may hold values from -0.1875 to 0.1875
Outputs:
- layer_out: bfloat16 [3072, 2048], P('sp', 'tp')
Inputs may be any that keep to these rules, and one draw needn't show every extreme that they name: The logarithm of a per-position decay rate: exp(decay_log) lies between 0.1 / 3072 and 0.08. `expert_ids`: each row names 2 different experts. Among the rows of one index of sp (384 tokens) no expert is named more than 48 times, a bound that some block reaches there.
All inputs are finite; a program needn't handle non-finite values.
Results may differ from a plain program's by a relative error of at most 0.014.
Values may be sent and summed in bfloat16 or wider, within the bound.
No kernel may reach another device: no remote copies, remote signals or barrier semaphores. Data moves between devices by JAX's collectives and lax.ppermute only.
A program may use at most 64 MiB of HBM per device.

v0:
```python
import jax
import jax.numpy as jnp
from jax import lax
from jax.experimental import pallas as pl
from jax.experimental.pallas import tpu as pltpu
from jax.sharding import PartitionSpec as P

SPAN = 128
LEAD = 16
VMEM_LIMIT = 16 * 2**20
MIXER_LIMIT = 60 * 2**20
TOPK = 2
CAP = 48


EPS = 1e-06


def from_behind(value, axis, steps):
    count = lax.axis_size(axis)
    first, last = (max(0, -steps), min(count, count - steps))
    return lax.ppermute(value, axis, [(source, source + steps) for source in range(first, last)])


def silu(x):
    return x * (0.5 * jnp.tanh(0.5 * x) + 0.5)


def swap_core(value):
    count = lax.axis_size("sp")
    return lax.ppermute(value, "sp", [(i, i ^ 1) for i in range(count)])


def move_chips(value, steps, cross=False):
    count = lax.axis_size("sp")
    return lax.ppermute(
        value, "sp", [(i, ((i + 2 * steps) % count) ^ int(cross)) for i in range(count)]
    )


def swap_tp(value, mask):
    count = lax.axis_size("tp")
    return lax.ppermute(value, "tp", [(i, i ^ mask) for i in range(count)])


def gather_tp(rows, mask):
    count = lax.axis_size("tp")
    if count != 4:
        every = lax.all_gather(rows, "tp")
        own = lax.axis_index("tp")
        return [lax.dynamic_index_in_dim(every, own ^ m, 0, False) for m in range(count)]
    near = swap_tp(rows, mask)
    other = swap_tp(rows, 3 - mask)
    far = swap_tp(near, 3 - mask)
    return [rows, near, other, far] if mask == 1 else [rows, other, near, far]


def routing_tables(ids, weights, own, experts):
    blocks = ids.shape[0] // TOPK
    tokens = ids.shape[1]
    shape = (blocks, experts, tokens)

    def kernel(own_ref, ids_ref, weight_ref, arrive_ref, leave_ref, share_ref):
        expert = lax.broadcasted_iota(jnp.int32, (experts, tokens), 0)
        first = own_ref[0] * experts
        named = []
        for b in range(blocks):
            rows = [ids_ref[TOPK * b + j : TOPK * b + j + 1] for j in range(TOPK)]
            named.append(sum((row == expert + first).astype(jnp.float32) for row in rows))
        own_rows = [ids_ref[j : j + 1] for j in range(TOPK)]
        for b in range(blocks):
            owner = ((own_ref[0] + 2 * (b // 2)) % blocks) ^ (b % 2)
            hits = [(row == expert + owner * experts).astype(jnp.float32) for row in own_rows]
            named.append(sum(hits))
            share_ref[b] = sum(hit * weight_ref[j : j + 1] for j, hit in enumerate(hits))
        every = jnp.concatenate(named, axis=0)
        row = lax.broadcasted_iota(jnp.int32, (tokens, tokens), 0)
        column = lax.broadcasted_iota(jnp.int32, (tokens, tokens), 1)
        slots = dot32(every.astype(jnp.bfloat16), (row < column).astype(jnp.bfloat16))
        slots = jnp.where(every > 0, slots.astype(jnp.int32), -1)
        for b in range(blocks):
            arrive_ref[b] = slots[b * experts : (b + 1) * experts]
            leave_ref[b] = slots[(blocks + b) * experts : (blocks + b + 1) * experts]

    return pl.pallas_call(
        kernel,
        in_specs=[
            pl.BlockSpec(memory_space=pltpu.SMEM), pl.BlockSpec(memory_space=pltpu.VMEM),
            pl.BlockSpec(memory_space=pltpu.VMEM),
        ],
        out_shape=[
            jax.ShapeDtypeStruct(shape, jnp.int32), jax.ShapeDtypeStruct(shape, jnp.int32),
            jax.ShapeDtypeStruct(shape, jnp.float32),
        ],
        compiler_params=pltpu.CompilerParams(vmem_limit_bytes=VMEM_LIMIT),
        name="routing_tables",
    )(own, ids, weights)


def pick_rows(blocks, ranks, places):
    experts = ranks.shape[1]
    tokens, width = blocks[0].shape
    count = len(blocks)

    def kernel(*refs):
        block_refs, rank_ref, out_ref = refs[:count], refs[count], refs[-1]
        slot = lax.broadcasted_iota(jnp.int32, (CAP, tokens), 0)
        for side, rows in enumerate(block_refs):
            rank = rank_ref[places[side]]
            chosen = jnp.concatenate(
                [(rank[e : e + 1, :] == slot).astype(jnp.float32) for e in range(experts)], axis=0
            ).astype(jnp.bfloat16)
            picked = dot32(chosen, rows[...]).astype(jnp.bfloat16)
            for e in range(experts):
                out_ref[e, side] = picked[e * CAP : (e + 1) * CAP]

    return pl.pallas_call(
        kernel,
        out_shape=jax.ShapeDtypeStruct((experts, count, CAP, width), jnp.bfloat16),
        cost_estimate=pl.CostEstimate(
            flops=2 * count * experts * CAP * tokens * width,
            bytes_accessed=4 * count * tokens * width,
            transcendentals=0,
        ),
        compiler_params=pltpu.CompilerParams(vmem_limit_bytes=VMEM_LIMIT),
        name="pick_rows",
    )(*blocks, ranks)


def hidden_units(pieces, gate, up, inverse, own):
    experts, full, units = gate.shape
    rows, width = pieces[0].shape
    each = rows // experts
    count = len(pieces)
    lanes = inverse.shape[1]

    def kernel(own_ref, *refs):
        parts, (gate_ref, up_ref, inverse_ref, out_ref) = refs[:count], refs[count:]
        gate_sum = jnp.zeros((each, units), jnp.float32)
        up_sum = jnp.zeros((each, units), jnp.float32)
        squares = jnp.zeros((each, lanes), jnp.float32)
        for m in range(count):
            part = parts[m][...]
            at = pl.ds(pl.multiple_of((own_ref[0] ^ m) * width, width), width)
            gate_sum += dot32(part, gate_ref[0, at, :])
            up_sum += dot32(part, up_ref[0, at, :])
            squares += dot32(part * part, inverse_ref[at, :])
        scale = lax.rsqrt(squares[:, :1] / full + EPS)
        out_ref[...] = (silu(gate_sum * scale) * (up_sum * scale)).astype(jnp.bfloat16)

    return pl.pallas_call(
        kernel,
        grid_spec=pltpu.PrefetchScalarGridSpec(
            num_scalar_prefetch=1,
            grid=(experts,),
            in_specs=[pl.BlockSpec((each, width), lambda e, o: (e, 0)) for _ in range(count)]
            + [pl.BlockSpec((1, full, units), lambda e, o: (e, 0, 0)) for _ in range(2)]
            + [pl.BlockSpec((full, lanes), lambda e, o: (0, 0))],
            out_specs=pl.BlockSpec((each, units), lambda e, o: (e, 0)),
        ),
        out_shape=jax.ShapeDtypeStruct((rows, units), jnp.bfloat16),
        cost_estimate=pl.CostEstimate(
            flops=4 * rows * full * units,
            bytes_accessed=4 * experts * full * units,
            transcendentals=rows * units,
        ),
        compiler_params=pltpu.CompilerParams(vmem_limit_bytes=VMEM_LIMIT),
        name="hidden_units",
    )(own, *pieces, gate, up, inverse)


def expert_rows(pieces, down, own):
    experts, full, columns = down.shape
    rows, units = pieces[0].shape
    each = rows // experts
    blocks = each // CAP
    count = len(pieces)

    def kernel(own_ref, *refs):
        parts, down_ref, outs = refs[:count], refs[count], refs[count + 1 :]
        total = jnp.zeros((each, columns), jnp.float32)
        for m in range(count):
            at = pl.ds(pl.multiple_of((own_ref[0] ^ m) * units, units), units)
            total += dot32(parts[m][...], down_ref[0, at, :])
        for i in range(blocks):
            outs[i][...] = total[i * CAP : (i + 1) * CAP].astype(jnp.bfloat16)

    return pl.pallas_call(
        kernel,
        grid_spec=pltpu.PrefetchScalarGridSpec(
            num_scalar_prefetch=1,
            grid=(experts,),
            in_specs=[pl.BlockSpec((each, units), lambda e, o: (e, 0)) for _ in range(count)]
            + [pl.BlockSpec((1, full, columns), lambda e, o: (e, 0, 0))],
            out_specs=[pl.BlockSpec((CAP, columns), lambda e, o: (e, 0)) for _ in range(blocks)],
        ),
        out_shape=[jax.ShapeDtypeStruct((experts * CAP, columns), jnp.bfloat16) for _ in range(blocks)],
        cost_estimate=pl.CostEstimate(
            flops=2 * rows * full * columns,
            bytes_accessed=2 * experts * full * columns,
            transcendentals=0,
        ),
        compiler_params=pltpu.CompilerParams(vmem_limit_bytes=VMEM_LIMIT),
        name="expert_rows",
    )(own, *pieces, down)


def combine(total, returned, places, ranks, shares, kind):
    tokens, columns = total.shape
    count = len(returned)
    experts = ranks.shape[1]

    def kernel(total_ref, *refs):
        rows_refs, rank_ref, share_ref, out_ref = refs[:count], refs[-3], refs[-2], refs[-1]
        slot = lax.broadcasted_iota(jnp.int32, (CAP, tokens), 0)
        value = total_ref[...]
        for place, rows in zip(places, rows_refs):
            rank, share = rank_ref[place], share_ref[place]
            chosen = jnp.concatenate(
                [
                    jnp.where(rank[e : e + 1, :] == slot, share[e : e + 1, :], 0.0)
                    for e in range(experts)
                ],
                axis=0,
            )
            for part in halves(chosen):
                value += lax.dot_general(
                    part, rows[...], (((0,), (0,)), ((), ())), preferred_element_type=jnp.float32
                )
        out_ref[...] = value.astype(kind)

    return pl.pallas_call(
        kernel,
        out_shape=jax.ShapeDtypeStruct((tokens, columns), kind),
        cost_estimate=pl.CostEstimate(
            flops=4 * count * tokens * experts * CAP * columns,
            bytes_accessed=8 * tokens * columns,
            transcendentals=0,
        ),
        compiler_params=pltpu.CompilerParams(vmem_limit_bytes=VMEM_LIMIT),
        name="combine",
    )(total, *returned, ranks, shares)


def halves(value):
    high = value.astype(jnp.bfloat16)
    return high, (value - high.astype(jnp.float32)).astype(jnp.bfloat16)


def column(row):
    size = row.shape[1]
    same = lax.broadcasted_iota(jnp.int32, (size, size), 0) == lax.broadcasted_iota(
        jnp.int32, (size, size), 1
    )
    return jnp.sum(jnp.where(same, row, 0.0), axis=1, keepdims=True)


def dot32(left, right):
    return jnp.dot(left, right, preferred_element_type=jnp.float32)


def to_channels(value, group, per_group, channels):
    heads = value.shape[0]
    row = lax.broadcasted_iota(jnp.int32, (heads, channels), 0)
    column = lax.broadcasted_iota(jnp.int32, (heads, channels), 1)
    spread = (row == group * per_group + column // (channels // per_group)).astype(jnp.bfloat16)
    high, low = halves(value)
    over = (((0,), (0,)), ((), ()))
    return lax.dot_general(
        high, spread, over, preferred_element_type=jnp.float32
    ) + lax.dot_general(low, spread, over, preferred_element_type=jnp.float32)


def of_group(taps, group):
    place = lax.broadcasted_iota(jnp.int32, taps.shape, 1)
    return jnp.sum(jnp.where(place == group, taps[...].astype(jnp.float32), 0.0), axis=1)


def convolve(halo, rows, taps, scratch):
    lead, length = halo.shape[0], rows.shape[0]
    weights = taps.astype(jnp.float32)
    count = weights.shape[0]
    scratch[:lead] = halo[...].astype(jnp.float32)
    scratch[lead:] = rows[...].astype(jnp.float32)
    total = weights[0:1] * scratch[lead - count + 1 : lead - count + 1 + length]
    for k in range(1, count):
        total += weights[k : k + 1] * scratch[lead - count + 1 + k : lead - count + 1 + k + length]
    return silu(total)


def mixer_states(act, writes, halo, taps, write_taps, raw, bias, decay, groups, span):
    heads, length = raw.shape
    channels, state = act.shape[1] // groups, write_taps.shape[2]
    per_group = heads // groups
    blocks = length // span
    lead = halo.shape[0]
    skip = act.shape[1] // state

    def kernel(act_ref, write_ref, halo_ref, halo_w_ref, taps_ref, taps_w_ref, raw_ref, bias_ref,
               decay_ref, value_ref, out_w_ref, cum_ref, sum_ref, enter_ref, close_ref, scale_ref,
               pad_ref, pad_w_ref):
        group = pl.program_id(0)

        @pl.when(group == 0)
        def _():
            x = raw_ref[...].astype(jnp.float32) + column(bias_ref[...])
            step = jnp.maximum(x, 0.0) + jnp.log1p(jnp.exp(-jnp.abs(x)))
            logs = step * -jnp.exp(column(decay_ref[...]))
            row = lax.broadcasted_iota(jnp.int32, (span, span), 0)
            upto = (row <= lax.broadcasted_iota(jnp.int32, (span, span), 1)).astype(jnp.bfloat16)
            base = jnp.zeros((heads, 1), jnp.float32)
            for b in range(blocks):
                at = slice(b * span, (b + 1) * span)
                part = logs[:, at]
                high, low = halves(part)
                rest = (part - high.astype(jnp.float32) - low.astype(jnp.float32)).astype(jnp.bfloat16)
                cum = dot32(high, upto) + dot32(low, upto) + dot32(rest, upto)
                cum_ref[:, at] = cum
                sum_ref[:, at] = cum + base
                scale_ref[:, at] = step[:, at] * jnp.exp(-cum)
                base = base + cum[:, span - 1 : span]

        values = convolve(halo_ref, act_ref, taps_ref[...], pad_ref)
        scaled = values * to_channels(scale_ref[...], group, per_group, channels)
        value_ref[...] = scaled.astype(jnp.bfloat16)
        out_w_ref[...] = convolve(
            halo_w_ref, write_ref, of_group(taps_w_ref, group), pad_w_ref
        ).astype(jnp.bfloat16)
        carried = jnp.zeros((state, channels), jnp.float32)
        place = lax.broadcasted_iota(jnp.int32, (heads, 8), 1)
        lasts = sum_ref[:, length - 1 :]
        for b in range(blocks):
            lasts = jnp.where(place == b, cum_ref[:, (b + 1) * span - 1 : (b + 1) * span], lasts)
        ends = to_channels(jnp.exp(lasts), group, per_group, channels)
        for b in range(blocks):
            enter_ref[b * state : (b + 1) * state] = carried.astype(jnp.bfloat16)
            here = lax.dot_general(
                out_w_ref[b * span : (b + 1) * span], value_ref[b * span : (b + 1) * span],
                (((0,), (0,)), ((), ())), preferred_element_type=jnp.float32,
            )
            carried = ends[b : b + 1] * (carried + here)
        close_ref[:state] = carried.astype(jnp.bfloat16)
        close_ref[state:] = jnp.broadcast_to(ends[7:8], (16, channels)).astype(jnp.bfloat16)

    by_group = lambda rows, width: pl.BlockSpec((rows, width), lambda g: (0, g))
    whole = lambda rows, width: pl.BlockSpec((rows, width), lambda g: (0, 0))
    return pl.pallas_call(
        kernel,
        grid=(groups,),
        in_specs=[
            by_group(length, channels), by_group(length, state),
            by_group(lead, channels), pl.BlockSpec((lead, state), lambda g: (0, skip + g)),
            by_group(taps.shape[0], channels), pl.BlockSpec(write_taps.shape, lambda g: (0, 0, 0)),
            whole(heads, length), whole(1, heads), whole(1, heads),
        ],
        out_specs=[
            by_group(length, channels), by_group(length, state), whole(heads, length),
            whole(heads, length), by_group(blocks * state, channels), by_group(state + 16, channels),
        ],
        out_shape=[
            jax.ShapeDtypeStruct((length, groups * channels), jnp.bfloat16),
            jax.ShapeDtypeStruct((length, groups * state), jnp.bfloat16),
            jax.ShapeDtypeStruct((heads, length), jnp.float32),
            jax.ShapeDtypeStruct((heads, length), jnp.float32),
            jax.ShapeDtypeStruct((blocks * state, groups * channels), jnp.bfloat16),
            jax.ShapeDtypeStruct((state + 16, groups * channels), jnp.bfloat16),
        ],
        scratch_shapes=[
            pltpu.VMEM((heads, length), jnp.float32),
            pltpu.VMEM((lead + length, channels), jnp.float32),
            pltpu.VMEM((lead + length, state), jnp.float32),
        ],
        compiler_params=pltpu.CompilerParams(dimension_semantics=("arbitrary",), vmem_limit_bytes=MIXER_LIMIT),
        name="mixer_states",
    )(act, writes, halo, halo, taps, write_taps, raw, bias, decay)


def mixer_local(reads, halo, read_taps, values, writes, entering, cum, groups, span):
    heads, length = cum.shape
    channels, state = values.shape[1] // groups, read_taps.shape[2]
    per_group = heads // groups
    blocks = length // span
    lead = halo.shape[0]
    skip = values.shape[1] // state + groups

    def kernel(read_ref, halo_ref, taps_ref, value_ref, write_ref, enter_ref, cum_ref, out_ref,
               out_r_ref, pad_ref):
        group = pl.program_id(0)
        out_r_ref[...] = convolve(
            halo_ref, read_ref, of_group(taps_ref, group), pad_ref
        ).astype(jnp.bfloat16)
        grown = to_channels(jnp.exp(cum_ref[...]), group, per_group, channels)
        row = lax.broadcasted_iota(jnp.int32, (span, span), 0)
        column = lax.broadcasted_iota(jnp.int32, (span, span), 1)
        for b in range(blocks):
            at = slice(b * span, (b + 1) * span)
            meet = lax.dot_general(
                out_r_ref[at], write_ref[at], (((1,), (1,)), ((), ())),
                preferred_element_type=jnp.float32,
            )
            meet = jnp.where(row >= column, meet, 0.0).astype(jnp.bfloat16)
            total = dot32(meet, value_ref[at])
            if b:
                total += dot32(out_r_ref[at], enter_ref[b * state : (b + 1) * state])
            out_ref[at] = grown[at] * total

    by_group = lambda rows, width: pl.BlockSpec((rows, width), lambda g: (0, g))
    return pl.pallas_call(
        kernel,
        grid=(groups,),
        in_specs=[
            pl.BlockSpec((length, state), lambda g: (0, groups + g)),
            pl.BlockSpec((lead, state), lambda g: (0, skip + g)), pl.BlockSpec(read_taps.shape, lambda g: (0, 0, 0)), by_group(length, channels),
            by_group(length, state), by_group(blocks * state, channels),
            pl.BlockSpec((heads, length), lambda g: (0, 0)),
        ],
        out_specs=[by_group(length, channels), by_group(length, state)],
        out_shape=[
            jax.ShapeDtypeStruct((length, groups * channels), jnp.float32),
            jax.ShapeDtypeStruct((length, groups * state), jnp.bfloat16),
        ],
        scratch_shapes=[pltpu.VMEM((lead + length, state), jnp.float32)],
        compiler_params=pltpu.CompilerParams(dimension_semantics=("arbitrary",), vmem_limit_bytes=MIXER_LIMIT),
        cost_estimate=pl.CostEstimate(
            flops=4 * 10**9, bytes_accessed=4 * 10**6, transcendentals=length * groups * state
        ),
        name="mixer_local",
    )(reads, halo, read_taps, values, writes, entering, cum)


def mixer_project(local, reads, sums, arriving, gates, gain, weight, own, shares, groups):
    heads, length = sums.shape
    channels, state = local.shape[1] // groups, reads.shape[1] // groups
    per_group = heads // groups
    width = weight.shape[1] // shares

    def kernel(own_ref, local_ref, read_ref, sum_ref, arrive_ref, gate_ref, gain_ref, *refs):
        weights, outs = refs[:shares], refs[shares : 2 * shares]
        mixed_ref, kept_ref = refs[2 * shares :]
        group = pl.program_id(0)
        for m in range(shares):
            kept_ref[m, pl.ds(pl.multiple_of(group * channels, channels), channels)] = weights[m][...]
        grown = to_channels(jnp.exp(sum_ref[...]), group, per_group, channels)
        y = local_ref[...] + grown * dot32(read_ref[...], arrive_ref[...])
        gated = y * silu(gate_ref[...].astype(jnp.float32))
        row = lax.broadcasted_iota(jnp.int32, (channels, channels), 0) // (channels // per_group)
        column = lax.broadcasted_iota(jnp.int32, (channels, channels), 1) // (channels // per_group)
        same = jnp.where(row == column, per_group / channels, 0.0).astype(jnp.bfloat16)
        mean = dot32((gated * gated).astype(jnp.bfloat16), same)
        mixed_ref[group] = (gated * lax.rsqrt(mean + EPS) * gain_ref[...]).astype(jnp.bfloat16)

        @pl.when(group == groups - 1)
        def _():
            mixed = jnp.concatenate([mixed_ref[g] for g in range(groups)], axis=1)
            for m in reversed(range(shares)):
                outs[m][...] = dot32(mixed, kept_ref[m]).astype(jnp.bfloat16)

    by_group = lambda rows, width: pl.BlockSpec((rows, width), lambda g, o: (0, g))
    whole = lambda rows, width: pl.BlockSpec((rows, width), lambda g, o: (0, 0))
    share = lambda m: pl.BlockSpec((channels, width), lambda g, o: (g, o[0] ^ m))
    return pl.pallas_call(
        kernel,
        grid_spec=pltpu.PrefetchScalarGridSpec(
            num_scalar_prefetch=1,
            grid=(groups,),
            in_specs=[
                by_group(length, channels), by_group(length, state), whole(heads, length),
                by_group(state, channels), by_group(length, channels), by_group(1, channels),
            ]
            + [share(m) for m in range(shares)],
            out_specs=[whole(length, width) for _ in range(shares)],
            scratch_shapes=[
                pltpu.VMEM((groups, length, channels), jnp.bfloat16),
                pltpu.VMEM((shares, weight.shape[0], width), jnp.bfloat16),
            ],
        ),
        out_shape=[jax.ShapeDtypeStruct((length, width), jnp.bfloat16) for _ in range(shares)],
        compiler_params=pltpu.CompilerParams(dimension_semantics=("arbitrary",), vmem_limit_bytes=MIXER_LIMIT),
        name="mixer_project",
    )(own, local, reads, sums, arriving, gates, gain, *[weight] * shares)


def sent_states(closing, state):
    core = lax.axis_index("sp") % 2
    count = lax.axis_size("sp")
    half = closing.shape[1] // 2
    other = swap_core(closing)
    part = lambda rows: lax.dynamic_slice_in_dim(rows, core * half, half, 1).astype(jnp.float32)
    mine, theirs = part(closing), part(other)
    early = jnp.where(core == 0, mine, theirs)
    late = jnp.where(core == 0, theirs, mine)
    decay = late[state : state + 1]
    chip = jnp.concatenate([early[:state] * decay + late[:state], early[state:] * decay], axis=0)
    chip = chip.astype(jnp.bfloat16)
    sent = []
    for k in range(1, count // 2):
        pairs = [(i, i + 2 * k) for i in range(count - 2 * k)]
        sent.append(lax.ppermute(chip, "sp", pairs))
    return sent, other


def arriving_state(sent, other, state):
    core = lax.axis_index("sp") % 2
    total = jnp.zeros((state, sent[0].shape[1]), jnp.float32)
    for rows in reversed(sent):
        rows = rows.astype(jnp.float32)
        total = rows[:state] + rows[state : state + 1] * total
    total = total.astype(jnp.bfloat16)
    swapped = swap_core(total)
    low = jnp.where(core == 0, total, swapped)
    high = jnp.where(core == 0, swapped, total)
    both = jnp.concatenate([low, high], axis=1)
    before = other.astype(jnp.float32)
    after = before[:state] + before[state : state + 1] * both.astype(jnp.float32)
    return jnp.where(core == 0, both, after.astype(jnp.bfloat16))


def per_device(
    stream,
    inner_act,
    gate_act,
    state_write,
    state_read,
    step_raw,
    conv_inner,
    conv_write,
    conv_read,
    step_bias,
    decay_log,
    inner_gain,
    out_weight,
    ffn_gain,
    expert_ids,
    expert_weights,
    expert_gate,
    expert_up,
    expert_down,
):
    length = inner_act.shape[0]
    groups_here = state_write.shape[1]
    state_dim = state_write.shape[2]
    write_width = groups_here * state_dim
    tail_rows = [inner_act[length - LEAD :]]
    tail_rows += [a[length - LEAD :].reshape(LEAD, write_width) for a in (state_write, state_read)]
    halo = from_behind(jnp.concatenate(tail_rows, axis=1), "sp", 1)
    joined = jnp.concatenate(
        [a.reshape(length, write_width) for a in (state_write, state_read)], axis=1
    )
    own_tp = lax.axis_index("tp")
    own_sp = lax.axis_index("sp")
    own_index = own_tp.astype(jnp.int32).reshape(1)
    tp_count = lax.axis_size("tp")
    chips = lax.axis_size("sp") // 2
    values, writes, cum, sums, entering, closing = mixer_states(
        inner_act,
        joined,
        halo,
        conv_inner,
        conv_write,
        step_raw.T,
        step_bias[None],
        decay_log[None],
        groups_here,
        SPAN,
    )
    sent, other = sent_states(closing, state_dim)
    local, reads = mixer_local(
        joined,
        halo,
        conv_read,
        values,
        writes,
        entering,
        cum,
        groups_here,
        SPAN,
    )
    local_experts = expert_gate.shape[0]
    ids_own = expert_ids.T
    ids_other = swap_core(ids_own)
    ids_of = [jnp.concatenate([ids_own, ids_other], axis=0)]
    for k in range(1, chips):
        ids_of.append(move_chips(ids_of[0], k))
    arrive_ranks, leave_ranks, shares = routing_tables(
        jnp.concatenate(ids_of, axis=0),
        expert_weights.T,
        own_sp.astype(jnp.int32).reshape(1),
        local_experts,
    )
    out_width = expert_down.shape[2]
    own_start = own_tp * out_width
    share_of = lax.dynamic_slice_in_dim(stream, own_start, out_width, 1)
    gain_share = lax.dynamic_slice_in_dim(ffn_gain, own_start, out_width, 0)
    inverse = jnp.broadcast_to((1.0 / (ffn_gain * ffn_gain))[:, None], (ffn_gain.shape[0], 128))
    inverse = inverse.astype(jnp.bfloat16)
    arriving = arriving_state(sent, other, state_dim)
    leaving = mixer_project(
        local,
        reads,
        sums,
        arriving,
        gate_act,
        inner_gain[None],
        out_weight,
        own_index,
        tp_count,
        groups_here,
    )
    projected = leaving[0].astype(jnp.float32)
    for m in reversed(range(1, tp_count)):
        part = swap_tp(leaving[m], m)
        projected = projected + part.astype(jnp.float32)
    kept = share_of.astype(jnp.float32) + projected
    rows = (kept * gain_share[None, :]).astype(jnp.bfloat16)
    blocks_of = []
    for k in range(chips):
        if k:
            rows = move_chips(rows, 1)
        blocks_of.append([rows, swap_core(rows)])
    chunks = [[k] for k in range(chips)]
    returned = []
    for i, chunk in enumerate(chunks):
        mask, hidden_mask = RELAYS[i % 4]
        picked = pick_rows(
            [rows for k in chunk for rows in blocks_of[k]],
            arrive_ranks,
            [2 * k + side for k in chunk for side in range(2)],
        ).reshape(-1, out_width)
        pieces = gather_tp(picked, mask)
        hidden = hidden_units(pieces, expert_gate, expert_up, inverse, own_index)
        pieces = gather_tp(hidden, hidden_mask)
        given = expert_rows(pieces, expert_down, own_index)
        for j, k in enumerate(chunk):
            for side in range(2):
                home = given[2 * j + side]
                if k or side:
                    home = move_chips(home, -k, bool(side))
                returned.append((2 * k + side, home))
    returned = returned[2:-2] + returned[-2:] + returned[:2]
    late = 4
    total = kept
    for part, kind in ((returned[:-late], jnp.float32), (returned[-late:], jnp.bfloat16)):
        places, rows = zip(*part)
        total = combine(total, rows, places, leave_ranks, shares, kind)
    return total


RELAYS = ((2, 1), (1, 2), (2, 2), (1, 2))


def solution(mesh):
    return jax.shard_map(
        per_device,
        mesh=mesh,
        in_specs=(
            P("sp", None),
            P("sp", "tp"),
            P("sp", "tp"),
            P("sp", "tp", None),
            P("sp", "tp", None),
            P("sp", "tp"),
            P(None, "tp"),
            P(None, "tp", None),
            P(None, "tp", None),
            P("tp"),
            P("tp"),
            P("tp"),
            P("tp", None),
            P(),
            P("sp", None),
            P("sp", None),
            P("sp", None, "tp"),
            P("sp", None, "tp"),
            P("sp", None, "tp"),
        ),
        out_specs=P("sp", "tp"),
        check_vma=False,
    )
```

profile of v0, /device:TPU:0, one launch (start us, length us, event | category | flops | bytes accessed | tf_op | source)
XLA Modules:
  0.0 230.3 jit_solution(12999906842089182208)
XLA Ops:
  2.2 2.4 %collective-permute-start = (bf16[16,2048]{1,0:T(8,128)(2,1)S(1)}, bf16[16,2048]{1,0:T(8,128)(2,1)S(1)}, u32[]{:S(2)}, u32[]{:S(2)}) collective-permute-start(bf16[16,2048]{1,0:T(8,128)(2,1)S(1)} %pad_maximum_fusion.1), channel_id=1, source_target_pairs={{0,4},{4,8},{8,12},{12,16},{16,20},{20,24},{24,28},{1,5},{5,9},{9,... | collective-permute-start | bytes 196616 | tf_op jit(solution)/shard_map/ppermute | solution.py:22
  7.7 5.8 %mixer_states.1 = (bf16[384,1024]{1,0:T(8,128)(2,1)}, bf16[384,512]{1,0:T(8,128)(2,1)}, f32[16,384]{1,0:T(8,128)}, f32[16,384]{1,0:T(8,128)}, bf16[384,1024]{1,0:T(8,128)(2,1)}, /*index=5*/bf16[144,1024]{1,0:T(8,128)(2,1)}) custom-call(bf16[384,1024]{1,0:T(8,128)(2,1)} %act_ref.1, bf16[384,1024]{1,0:T(8,128)(2,1)} %copy-done.5, bf16[16,2048]{1,0:T(8,128)(2,1)} %copy-done.6, ...), custom_call_target="tpu_custom_call" | custom-call | tf_op jit(solution)/shard_map/mixer_states/pallas_call | solution.py:347
  13.5 2.7 %collective-permute-start.1 = (bf16[144,1024]{1,0:T(8,128)(2,1)}, bf16[144,1024]{1,0:T(8,128)(2,1)S(1)}, u32[]{:S(2)}, u32[]{:S(2)}) collective-permute-start(bf16[144,1024]{1,0:T(8,128)(2,1)} %get-tuple-element.35), channel_id=1, source_target_pairs={{0,4},{4,0},{8,12},{12,8},{16,20},{20,16},{24,28},{28,24},{1,5},{5... | collective-permute-start | bytes 884744 | tf_op jit(solution)/shard_map/ppermute | solution.py:31
  18.7 3.5 %collective-permute-start.2 = (bf16[144,512]{1,0:T(8,128)(2,1)S(1)}, bf16[144,512]{1,0:T(8,128)(2,1)S(1)}, u32[]{:S(2)}, u32[]{:S(2)}) collective-permute-start(bf16[144,512]{1,0:T(8,128)(2,1)S(1)} %pad_maximum_fusion), channel_id=1, source_target_pairs={{0,8},{4,12},{8,16},{12,20},{16,24},{20,28},{1,9},{5,13},{9,17},{1... | collective-permute-start | bytes 442376 | tf_op jit(solution)/shard_map/ppermute | solution.py:498
  22.2 3.3 %collective-permute-start.4 = (bf16[144,512]{1,0:T(8,128)(2,1)S(1)}, bf16[144,512]{1,0:T(8,128)(2,1)S(1)}, u32[]{:S(2)}, u32[]{:S(2)}) collective-permute-start(bf16[144,512]{1,0:T(8,128)(2,1)S(1)} %pad_maximum_fusion), channel_id=1, source_target_pairs={{0,24},{4,28},{1,25},{5,29},{2,26},{6,30},{3,27},{7,31}} | collective-permute-start | bytes 442376 | tf_op jit(solution)/shard_map/ppermute | solution.py:498
  25.5 1.9 collective-permute-start.3
  27.4 2.3 %collective-permute-done.4 = bf16[144,512]{1,0:T(8,128)(2,1)S(1)} collective-permute-done((bf16[144,512]{1,0:T(8,128)(2,1)S(1)}, bf16[144,512]{1,0:T(8,128)(2,1)S(1)}, u32[]{:S(2)}, u32[]{:S(2)}) %collective-permute-start.4) | collective-permute-done | bytes 147488 | tf_op jit(solution)/shard_map/ppermute | solution.py:498
  29.8 2.4 %collective-permute-done.3 = bf16[144,512]{1,0:T(8,128)(2,1)S(1)} collective-permute-done((bf16[144,512]{1,0:T(8,128)(2,1)S(1)}, bf16[144,512]{1,0:T(8,128)(2,1)S(1)}, u32[]{:S(2)}, u32[]{:S(2)}) %collective-permute-start.3) | collective-permute-done | bytes 147488 | tf_op jit(solution)/shard_map/ppermute | solution.py:498
  32.4 5.9 %mixer_local.1 = (f32[384,1024]{1,0:T(8,128)}, bf16[384,512]{1,0:T(8,128)(2,1)}) custom-call(bf16[384,1024]{1,0:T(8,128)(2,1)} %copy-done.5, bf16[16,2048]{1,0:T(8,128)(2,1)} %copy-done.6, bf16[4,4,128]{2,1,0:T(4,128)(2,1)} %taps_ref.3, bf16[384,1024]{1,0:T(8,128)(2,1)} %get-tuple-element.28.value_ref, bf16[384,512]{1,0:T(8,128)(2,1)} %get-tuple-element.29.write_ref, ...), custom_call_target="tpu_custom_call" | custom-call | flops 4000000000 | bytes 4000000 | tf_op jit(solution)/shard_map/mixer_local/pallas_call | solution.py:408
  39.2 8.5 %mixer_project.1 = (bf16[384,512]{1,0:T(8,128)(2,1)}, bf16[384,512]{1,0:T(8,128)(2,1)}, bf16[384,512]{1,0:T(8,128)(2,1)}, bf16[384,512]{1,0:T(8,128)(2,1)}) custom-call(s32[1]{0:T(128)} %bitcast.own_ref, f32[384,1024]{1,0:T(8,128)} %get-tuple-element.32.local_ref, bf16[384,512]{1,0:T(8,128)(2,1)} %get-tuple-element.33.read_ref, ...), custom_call_target="tpu_custom_call" | custom-call | tf_op jit(solution)/shard_map/mixer_project/pallas_call | solution.py:461
  47.7 2.5 %collective-permute-start.6 = (bf16[384,512]{1,0:T(8,128)(2,1)}, bf16[384,512]{1,0:T(8,128)(2,1)S(1)}, u32[]{:S(2)}, u32[]{:S(2)}) collective-permute-start(bf16[384,512]{1,0:T(8,128)(2,1)} %get-tuple-element.37), channel_id=1, source_target_pairs={{0,3},{1,2},{2,1},{3,0},{4,7},{5,6},{6,5},{7,4},{8,11},{9,10},{10,... | collective-permute-start | bytes 1179656 | tf_op jit(solution)/shard_map/ppermute | solution.py:43
  51.3 9.6 %collective-permute-done.6 = bf16[384,512]{1,0:T(8,128)(2,1)S(1)} collective-permute-done((bf16[384,512]{1,0:T(8,128)(2,1)}, bf16[384,512]{1,0:T(8,128)(2,1)S(1)}, u32[]{:S(2)}, u32[]{:S(2)}) %collective-permute-start.6) | collective-permute-done | bytes 393248 | tf_op jit(solution)/shard_map/ppermute | solution.py:43
  60.9 7.9 %collective-permute-done.7 = bf16[384,512]{1,0:T(8,128)(2,1)S(1)} collective-permute-done((bf16[384,512]{1,0:T(8,128)(2,1)}, bf16[384,512]{1,0:T(8,128)(2,1)S(1)}, u32[]{:S(2)}, u32[]{:S(2)}) %collective-permute-start.7) | collective-permute-done | bytes 393248 | tf_op jit(solution)/shard_map/ppermute | solution.py:43
  70.2 4.8 %collective-permute-start.9 = (bf16[384,512]{1,0:T(8,128)(2,1)S(1)}, bf16[384,512]{1,0:T(8,128)(2,1)S(1)}, u32[]{:S(2)}, u32[]{:S(2)}) collective-permute-start(bf16[384,512]{1,0:T(8,128)(2,1)S(1)} %get-tuple-element.51.refs_0_), channel_id=1, source_target_pairs={{0,8},{4,12},{8,16},{12,20},{16,24},{20,28},{24,0},{28,4},{1,9},{5... | collective-permute-start | bytes 1179656 | tf_op jit(solution)/shard_map/ppermute | solution.py:36
  75.0 12.0 %collective-permute-done.9.refs_0_ = bf16[384,512]{1,0:T(8,128)(2,1)S(1)} collective-permute-done((bf16[384,512]{1,0:T(8,128)(2,1)S(1)}, bf16[384,512]{1,0:T(8,128)(2,1)S(1)}, u32[]{:S(2)}, u32[]{:S(2)}) %collective-permute-start.9) | collective-permute-done | bytes 393248 | tf_op jit(solution)/shard_map/ppermute | solution.py:36
  87.0 12.2 %collective-permute-done.23.refs_0_ = bf16[384,512]{1,0:T(8,128)(2,1)S(1)} collective-permute-done((bf16[384,512]{1,0:T(8,128)(2,1)S(1)}, bf16[384,512]{1,0:T(8,128)(2,1)S(1)}, u32[]{:S(2)}, u32[]{:S(2)}) %collective-permute-start.23) | collective-permute-done | bytes 393248 | tf_op jit(solution)/shard_map/ppermute | solution.py:36
  101.0 4.4 %collective-permute-start.13 = (s32[4,384]{1,0:T(4,128)S(1)}, s32[4,384]{1,0:T(4,128)S(1)}, u32[]{:S(2)}, u32[]{:S(2)}) collective-permute-start(s32[4,384]{1,0:T(4,128)S(1)} %pad_add_fusion), channel_id=1, source_target_pairs={{0,16},{4,20},{8,24},{12,28},{16,0},{20,4},{24,8},{28,12},{1,17},{... | collective-permute-start | bytes 18440 | tf_op jit(solution)/shard_map/ppermute | solution.py:36
  105.4 5.5 %collective-permute-done.12 = s32[4,384]{1,0:T(4,128)S(1)} collective-permute-done((s32[4,384]{1,0:T(4,128)S(1)}, s32[4,384]{1,0:T(4,128)S(1)}, u32[]{:S(2)}, u32[]{:S(2)}) %collective-permute-start.12) | collective-permute-done | bytes 6176 | tf_op jit(solution)/shard_map/ppermute | solution.py:36
  110.9 3.5 %collective-permute-done.14 = s32[4,384]{1,0:T(4,128)S(1)} collective-permute-done((s32[4,384]{1,0:T(4,128)S(1)}, s32[4,384]{1,0:T(4,128)S(1)}, u32[]{:S(2)}, u32[]{:S(2)}) %collective-permute-start.14) | collective-permute-done | bytes 6176 | tf_op jit(solution)/shard_map/ppermute | solution.py:36
  115.2 1.6 collective-permute-start.15
  118.0 1.7 collective-permute-start.44
  120.3 6.9 %collective-permute-done.15.refs_1_ = bf16[384,512]{1,0:T(8,128)(2,1)S(1)} collective-permute-done((bf16[384,512]{1,0:T(8,128)(2,1)S(1)}, bf16[384,512]{1,0:T(8,128)(2,1)S(1)}, u32[]{:S(2)}, u32[]{:S(2)}) %collective-permute-start.15) | collective-permute-done | bytes 393248 | tf_op jit(solution)/shard_map/ppermute | solution.py:43
  127.2 1.7 collective-permute-start.26
  129.6 1.6 collective-permute-start.35
  131.2 4.5 %collective-permute-done.44.refs_1_ = bf16[384,512]{1,0:T(8,128)(2,1)S(1)} collective-permute-done((bf16[384,512]{1,0:T(8,128)(2,1)S(1)}, bf16[384,512]{1,0:T(8,128)(2,1)S(1)}, u32[]{:S(2)}, u32[]{:S(2)}) %collective-permute-start.44) | collective-permute-done | bytes 393248 | tf_op jit(solution)/shard_map/ppermute | solution.py:43
  138.3 7.9 %collective-permute-done.26.refs_2_ = bf16[384,512]{1,0:T(8,128)(2,1)S(1)} collective-permute-done((bf16[384,512]{1,0:T(8,128)(2,1)S(1)}, bf16[384,512]{1,0:T(8,128)(2,1)S(1)}, u32[]{:S(2)}, u32[]{:S(2)}) %collective-permute-start.26) | collective-permute-done | bytes 393248 | tf_op jit(solution)/shard_map/ppermute | solution.py:43
  146.8 7.8 %collective-permute-done.17.refs_3_ = bf16[384,512]{1,0:T(8,128)(2,1)S(1)} collective-permute-done((bf16[384,512]{1,0:T(8,128)(2,1)S(1)}, bf16[384,512]{1,0:T(8,128)(2,1)S(1)}, u32[]{:S(2)}, u32[]{:S(2)}) %collective-permute-start.17) | collective-permute-done | bytes 393248 | tf_op jit(solution)/shard_map/ppermute | solution.py:43
  155.2 1.7 collective-permute-start.37
  157.3 2.2 copy-done.2
  159.5 2.7 %hidden_units.4.refs_0_ = bf16[384,256]{1,0:T(8,128)(2,1)S(1)} custom-call(s32[1]{0:T(128)} %bitcast.own_ref, bf16[384,512]{1,0:T(8,128)(2,1)S(1)} %bitcast.34, bf16[384,512]{1,0:T(8,128)(2,1)S(1)} %collective-permute-done.15.refs_1_, bf16[384,512]{1,0:T(8,128)(2,1)S(1)} %collective-permute-done.16.refs_2_, ...), custom_call_target="tpu_custom_call" | custom-call | flops 805306368 | bytes 8388608 | tf_op jit(solution)/shard_map/hidden_units/pallas_call | solution.py:151
  162.6 2.7 %hidden_units.7.refs_0_ = bf16[384,256]{1,0:T(8,128)(2,1)S(1)} custom-call(s32[1]{0:T(128)} %bitcast.own_ref, bf16[384,512]{1,0:T(8,128)(2,1)S(1)} %bitcast.40, bf16[384,512]{1,0:T(8,128)(2,1)S(1)} %collective-permute-done.44.refs_1_, bf16[384,512]{1,0:T(8,128)(2,1)S(1)} %collective-permute-done.45.refs_2_, ...), custom_call_target="tpu_custom_call" | custom-call | flops 805306368 | bytes 8388608 | tf_op jit(solution)/shard_map/hidden_units/pallas_call | solution.py:151
  165.4 1.6 collective-permute-start.47
  166.9 2.4 %collective-permute-done.27.refs_3_ = bf16[384,512]{1,0:T(8,128)(2,1)S(1)} collective-permute-done((bf16[384,512]{1,0:T(8,128)(2,1)S(1)}, bf16[384,512]{1,0:T(8,128)(2,1)S(1)}, u32[]{:S(2)}, u32[]{:S(2)}) %collective-permute-start.27) | collective-permute-done | bytes 393248 | tf_op jit(solution)/shard_map/ppermute | solution.py:43
  169.4 1.7 collective-permute-start.48
  171.1 2.7 %hidden_units.5.refs_0_ = bf16[384,256]{1,0:T(8,128)(2,1)S(1)} custom-call(s32[1]{0:T(128)} %bitcast.own_ref, bf16[384,512]{1,0:T(8,128)(2,1)S(1)} %bitcast.37, bf16[384,512]{1,0:T(8,128)(2,1)S(1)} %collective-permute-done.25.refs_1_, bf16[384,512]{1,0:T(8,128)(2,1)S(1)} %collective-permute-done.26.refs_2_, ...), custom_call_target="tpu_custom_call" | custom-call | flops 805306368 | bytes 8388608 | tf_op jit(solution)/shard_map/hidden_units/pallas_call | solution.py:151
  173.8 1.9 collective-permute-done.19.refs_2_
  176.3 1.7 collective-permute-start.18
  178.3 2.7 %hidden_units.6.refs_0_ = bf16[384,256]{1,0:T(8,128)(2,1)S(1)} custom-call(s32[1]{0:T(128)} %bitcast.own_ref, bf16[384,512]{1,0:T(8,128)(2,1)S(1)} %bitcast.31, bf16[384,512]{1,0:T(8,128)(2,1)S(1)} %collective-permute-done.35.refs_1_, bf16[384,512]{1,0:T(8,128)(2,1)S(1)} %collective-permute-done.36.refs_2_, ...), custom_call_target="tpu_custom_call" | custom-call | flops 805306368 | bytes 8388608 | tf_op jit(solution)/shard_map/hidden_units/pallas_call | solution.py:151
  184.6 1.8 collective-permute-start.49
  186.4 1.9 collective-permute-done.20.refs_3_
  188.3 1.7 collective-permute-start.38
  192.5 1.8 collective-permute-start.21
  194.3 2.4 %collective-permute-done.30.refs_3_ = bf16[384,256]{1,0:T(8,128)(2,1)S(1)} collective-permute-done((bf16[384,256]{1,0:T(8,128)(2,1)S(1)}, bf16[384,256]{1,0:T(8,128)(2,1)S(1)}, u32[]{:S(2)}, u32[]{:S(2)}) %collective-permute-start.30) | collective-permute-done | bytes 196640 | tf_op jit(solution)/shard_map/ppermute | solution.py:43
  198.1 2.5 %collective-permute-done.38.refs_1_ = bf16[384,256]{1,0:T(8,128)(2,1)S(1)} collective-permute-done((bf16[384,256]{1,0:T(8,128)(2,1)S(1)}, bf16[384,256]{1,0:T(8,128)(2,1)S(1)}, u32[]{:S(2)}, u32[]{:S(2)}) %collective-permute-start.38) | collective-permute-done | bytes 196640 | tf_op jit(solution)/shard_map/ppermute | solution.py:43
  200.5 1.7 collective-permute-start.32
  206.1 17.0 %collective-permute-done.31.refs_2_ = bf16[192,512]{1,0:T(8,128)(2,1)S(1)} collective-permute-done((bf16[192,512]{1,0:T(8,128)(2,1)S(1)}, bf16[192,512]{1,0:T(8,128)(2,1)S(1)}, u32[]{:S(2)}, u32[]{:S(2)}) %collective-permute-start.31) | collective-permute-done | bytes 196640 | tf_op jit(solution)/shard_map/ppermute | solution.py:36
  223.1 4.3 %collective-permute-done.32.refs_3_ = bf16[192,512]{1,0:T(8,128)(2,1)S(1)} collective-permute-done((bf16[192,512]{1,0:T(8,128)(2,1)S(1)}, bf16[192,512]{1,0:T(8,128)(2,1)S(1)}, u32[]{:S(2)}, u32[]{:S(2)}) %collective-permute-start.32) | collective-permute-done | bytes 196640 | tf_op jit(solution)/shard_map/ppermute | solution.py:36
  228.5 1.8 combine.3
  (119 shorter events, 34.4 us)
Async XLA Ops:
  2.2 4.5 %collective-permute-start = (bf16[16,2048]{1,0:T(8,128)(2,1)S(1)}, bf16[16,2048]{1,0:T(8,128)(2,1)S(1)}, u32[]{:S(2)}, u32[]{:S(2)}) collective-permute-start(bf16[16,2048]{1,0:T(8,128)(2,1)S(1)} %pad_maximum_fusion.1), channel_id=1, source_target_pairs={{0,4},{4,8},{8,12},{12,16},{16,20},{20,24},{24,28},{1,5},{5,9},{9,... | collective-permute-start | bytes 196616 | tf_op jit(solution)/shard_map/ppermute | solution.py:22
  18.7 8.6 %collective-permute-start.2 = (bf16[144,512]{1,0:T(8,128)(2,1)S(1)}, bf16[144,512]{1,0:T(8,128)(2,1)S(1)}, u32[]{:S(2)}, u32[]{:S(2)}) collective-permute-start(bf16[144,512]{1,0:T(8,128)(2,1)S(1)} %pad_maximum_fusion), channel_id=1, source_target_pairs={{0,8},{4,12},{8,16},{12,20},{16,24},{20,28},{1,9},{5,13},{9,17},{1... | collective-permute-start | bytes 442376 | tf_op jit(solution)/shard_map/ppermute | solution.py:498
  22.2 7.5 %collective-permute-start.4 = (bf16[144,512]{1,0:T(8,128)(2,1)S(1)}, bf16[144,512]{1,0:T(8,128)(2,1)S(1)}, u32[]{:S(2)}, u32[]{:S(2)}) collective-permute-start(bf16[144,512]{1,0:T(8,128)(2,1)S(1)} %pad_maximum_fusion), channel_id=1, source_target_pairs={{0,24},{4,28},{1,25},{5,29},{2,26},{6,30},{3,27},{7,31}} | collective-permute-start | bytes 442376 | tf_op jit(solution)/shard_map/ppermute | solution.py:498
  25.5 6.7 %collective-permute-start.3 = (bf16[144,512]{1,0:T(8,128)(2,1)S(1)}, bf16[144,512]{1,0:T(8,128)(2,1)S(1)}, u32[]{:S(2)}, u32[]{:S(2)}) collective-permute-start(bf16[144,512]{1,0:T(8,128)(2,1)S(1)} %pad_maximum_fusion), channel_id=1, source_target_pairs={{0,16},{4,20},{8,24},{12,28},{1,17},{5,21},{9,25},{13,29},{2,18},{... | collective-permute-start | bytes 442376 | tf_op jit(solution)/shard_map/ppermute | solution.py:498
  32.3 6.0 %collective-permute-start.5 = (bf16[128,512]{1,0:T(8,128)(2,1)S(1)}, bf16[128,512]{1,0:T(8,128)(2,1)S(1)}, u32[]{:S(2)}, u32[]{:S(2)}) collective-permute-start(bf16[128,512]{1,0:T(8,128)(2,1)S(1)} %fusion.6), channel_id=1, source_target_pairs={{0,4},{4,0},{8,12},{12,8},{16,20},{20,16},{24,28},{28,24},{1,5},{5... | collective-permute-start | bytes 393224 | tf_op jit(solution)/shard_map/ppermute | solution.py:31
  47.7 13.1 %collective-permute-start.6 = (bf16[384,512]{1,0:T(8,128)(2,1)}, bf16[384,512]{1,0:T(8,128)(2,1)S(1)}, u32[]{:S(2)}, u32[]{:S(2)}) collective-permute-start(bf16[384,512]{1,0:T(8,128)(2,1)} %get-tuple-element.37), channel_id=1, source_target_pairs={{0,3},{1,2},{2,1},{3,0},{4,7},{5,6},{6,5},{7,4},{8,11},{9,10},{10,... | collective-permute-start | bytes 1179656 | tf_op jit(solution)/shard_map/ppermute | solution.py:43
  50.2 18.6 %collective-permute-start.7 = (bf16[384,512]{1,0:T(8,128)(2,1)}, bf16[384,512]{1,0:T(8,128)(2,1)S(1)}, u32[]{:S(2)}, u32[]{:S(2)}) collective-permute-start(bf16[384,512]{1,0:T(8,128)(2,1)} %get-tuple-element.38), channel_id=1, source_target_pairs={{0,2},{1,3},{2,0},{3,1},{4,6},{5,7},{6,4},{7,5},{8,10},{9,11},{10,... | collective-permute-start | bytes 1179656 | tf_op jit(solution)/shard_map/ppermute | solution.py:43
  50.7 18.2 %collective-permute-start.8 = (bf16[384,512]{1,0:T(8,128)(2,1)}, bf16[384,512]{1,0:T(8,128)(2,1)S(1)}, u32[]{:S(2)}, u32[]{:S(2)}) collective-permute-start(bf16[384,512]{1,0:T(8,128)(2,1)} %get-tuple-element.39), channel_id=1, source_target_pairs={{0,1},{1,0},{2,3},{3,2},{4,5},{5,4},{6,7},{7,6},{8,9},{9,8},{10,11... | collective-permute-start | bytes 1179656 | tf_op jit(solution)/shard_map/ppermute | solution.py:43
  70.2 16.8 %collective-permute-start.9 = (bf16[384,512]{1,0:T(8,128)(2,1)S(1)}, bf16[384,512]{1,0:T(8,128)(2,1)S(1)}, u32[]{:S(2)}, u32[]{:S(2)}) collective-permute-start(bf16[384,512]{1,0:T(8,128)(2,1)S(1)} %get-tuple-element.51.refs_0_), channel_id=1, source_target_pairs={{0,8},{4,12},{8,16},{12,20},{16,24},{20,28},{24,0},{28,4},{1,9},{5... | collective-permute-start | bytes 1179656 | tf_op jit(solution)/shard_map/ppermute | solution.py:36
  87.0 12.2 %collective-permute-start.23 = (bf16[384,512]{1,0:T(8,128)(2,1)S(1)}, bf16[384,512]{1,0:T(8,128)(2,1)S(1)}, u32[]{:S(2)}, u32[]{:S(2)}) collective-permute-start(bf16[384,512]{1,0:T(8,128)(2,1)S(1)} %collective-permute-done.9.refs_0_), channel_id=1, source_target_pairs={{0,8},{4,12},{8,16},{12,20},{16,24},{20,28},{24,0},{28,4},{1,9},{5... | collective-permute-start | bytes 1179656 | tf_op jit(solution)/shard_map/ppermute | solution.py:36
  87.0 27.8 %collective-permute-start.10 = (bf16[384,512]{1,0:T(8,128)(2,1)S(1)}, bf16[384,512]{1,0:T(8,128)(2,1)S(1)}, u32[]{:S(2)}, u32[]{:S(2)}) collective-permute-start(bf16[384,512]{1,0:T(8,128)(2,1)S(1)} %collective-permute-done.9.refs_0_), channel_id=1, source_target_pairs={{0,4},{4,0},{8,12},{12,8},{16,20},{20,16},{24,28},{28,24},{1,5},{5... | collective-permute-start | bytes 1179656 | tf_op jit(solution)/shard_map/ppermute | solution.py:31
  99.2 17.5 %collective-permute-start.33 = (bf16[384,512]{1,0:T(8,128)(2,1)S(1)}, bf16[384,512]{1,0:T(8,128)(2,1)S(1)}, u32[]{:S(2)}, u32[]{:S(2)}) collective-permute-start(bf16[384,512]{1,0:T(8,128)(2,1)S(1)} %collective-permute-done.23.refs_0_), channel_id=1, source_target_pairs={{0,8},{4,12},{8,16},{12,20},{16,24},{20,28},{24,0},{28,4},{1,9},{5... | collective-permute-start | bytes 1179656 | tf_op jit(solution)/shard_map/ppermute | solution.py:36
  99.2 17.8 %collective-permute-start.43 = (bf16[384,512]{1,0:T(8,128)(2,1)S(1)}, bf16[384,512]{1,0:T(8,128)(2,1)S(1)}, u32[]{:S(2)}, u32[]{:S(2)}) collective-permute-start(bf16[384,512]{1,0:T(8,128)(2,1)S(1)} %get-tuple-element.51.refs_0_), channel_id=1, source_target_pairs={{0,4},{4,0},{8,12},{12,8},{16,20},{20,16},{24,28},{28,24},{1,5},{5... | collective-permute-start | bytes 1179656 | tf_op jit(solution)/shard_map/ppermute | solution.py:31
  100.9 9.9 %collective-permute-start.12 = (s32[4,384]{1,0:T(4,128)S(1)}, s32[4,384]{1,0:T(4,128)S(1)}, u32[]{:S(2)}, u32[]{:S(2)}) collective-permute-start(s32[4,384]{1,0:T(4,128)S(1)} %pad_add_fusion), channel_id=1, source_target_pairs={{0,8},{4,12},{8,16},{12,20},{16,24},{20,28},{24,0},{28,4},{1,9},{5... | collective-permute-start | bytes 18440 | tf_op jit(solution)/shard_map/ppermute | solution.py:36
  101.0 9.9 %collective-permute-start.13 = (s32[4,384]{1,0:T(4,128)S(1)}, s32[4,384]{1,0:T(4,128)S(1)}, u32[]{:S(2)}, u32[]{:S(2)}) collective-permute-start(s32[4,384]{1,0:T(4,128)S(1)} %pad_add_fusion), channel_id=1, source_target_pairs={{0,16},{4,20},{8,24},{12,28},{16,0},{20,4},{24,8},{28,12},{1,17},{... | collective-permute-start | bytes 18440 | tf_op jit(solution)/shard_map/ppermute | solution.py:36
  114.7 4.9 %collective-permute-start.24 = (bf16[384,512]{1,0:T(8,128)(2,1)S(1)}, bf16[384,512]{1,0:T(8,128)(2,1)S(1)}, u32[]{:S(2)}, u32[]{:S(2)}) collective-permute-start(bf16[384,512]{1,0:T(8,128)(2,1)S(1)} %collective-permute-done.23.refs_0_), channel_id=1, source_target_pairs={{0,4},{4,0},{8,12},{12,8},{16,20},{20,16},{24,28},{28,24},{1,5},{5... | collective-permute-start | bytes 1179656 | tf_op jit(solution)/shard_map/ppermute | solution.py:31
  115.2 12.1 %collective-permute-start.15 = (bf16[384,512]{1,0:T(8,128)(2,1)S(1)}, bf16[384,512]{1,0:T(8,128)(2,1)S(1)}, u32[]{:S(2)}, u32[]{:S(2)}) collective-permute-start(bf16[384,512]{1,0:T(8,128)(2,1)S(1)} %bitcast.32), channel_id=1, source_target_pairs={{0,1},{1,0},{2,3},{3,2},{4,5},{5,4},{6,7},{7,6},{8,9},{9,8},{10,11... | collective-permute-start | bytes 1179656 | tf_op jit(solution)/shard_map/ppermute | solution.py:43
  116.7 12.2 %collective-permute-start.34 = (bf16[384,512]{1,0:T(8,128)(2,1)S(1)}, bf16[384,512]{1,0:T(8,128)(2,1)S(1)}, u32[]{:S(2)}, u32[]{:S(2)}) collective-permute-start(bf16[384,512]{1,0:T(8,128)(2,1)S(1)} %collective-permute-done.33.refs_0_), channel_id=1, source_target_pairs={{0,4},{4,0},{8,12},{12,8},{16,20},{20,16},{24,28},{28,24},{1,5},{5... | collective-permute-start | bytes 1179656 | tf_op jit(solution)/shard_map/ppermute | solution.py:31
  117.3 12.3 %collective-permute-start.45 = (bf16[384,512]{1,0:T(8,128)(2,1)S(1)}, bf16[384,512]{1,0:T(8,128)(2,1)S(1)}, u32[]{:S(2)}, u32[]{:S(2)}) collective-permute-start(bf16[384,512]{1,0:T(8,128)(2,1)S(1)} %bitcast.38), channel_id=1, source_target_pairs={{0,2},{1,3},{2,0},{3,1},{4,6},{5,7},{6,4},{7,5},{8,10},{9,11},{10,... | collective-permute-start | bytes 1179656 | tf_op jit(solution)/shard_map/ppermute | solution.py:43
  118.0 17.7 %collective-permute-start.44 = (bf16[384,512]{1,0:T(8,128)(2,1)S(1)}, bf16[384,512]{1,0:T(8,128)(2,1)S(1)}, u32[]{:S(2)}, u32[]{:S(2)}) collective-permute-start(bf16[384,512]{1,0:T(8,128)(2,1)S(1)} %bitcast.39), channel_id=1, source_target_pairs={{0,1},{1,0},{2,3},{3,2},{4,5},{5,4},{6,7},{7,6},{8,9},{9,8},{10,11... | collective-permute-start | bytes 1179656 | tf_op jit(solution)/shard_map/ppermute | solution.py:43
  119.6 18.2 %collective-permute-start.16 = (bf16[384,512]{1,0:T(8,128)(2,1)S(1)}, bf16[384,512]{1,0:T(8,128)(2,1)S(1)}, u32[]{:S(2)}, u32[]{:S(2)}) collective-permute-start(bf16[384,512]{1,0:T(8,128)(2,1)S(1)} %bitcast.33), channel_id=1, source_target_pairs={{0,2},{1,3},{2,0},{3,1},{4,6},{5,7},{6,4},{7,5},{8,10},{9,11},{10,... | collective-permute-start | bytes 1179656 | tf_op jit(solution)/shard_map/ppermute | solution.py:43
  127.2 19.0 %collective-permute-start.26 = (bf16[384,512]{1,0:T(8,128)(2,1)S(1)}, bf16[384,512]{1,0:T(8,128)(2,1)S(1)}, u32[]{:S(2)}, u32[]{:S(2)}) collective-permute-start(bf16[384,512]{1,0:T(8,128)(2,1)S(1)} %bitcast.35), channel_id=1, source_target_pairs={{0,2},{1,3},{2,0},{3,1},{4,6},{5,7},{6,4},{7,5},{8,10},{9,11},{10,... | collective-permute-start | bytes 1179656 | tf_op jit(solution)/shard_map/ppermute | solution.py:43
  129.0 25.7 %collective-permute-start.17 = (bf16[384,512]{1,0:T(8,128)(2,1)S(1)}, bf16[384,512]{1,0:T(8,128)(2,1)S(1)}, u32[]{:S(2)}, u32[]{:S(2)}) collective-permute-start(bf16[384,512]{1,0:T(8,128)(2,1)S(1)} %collective-permute-done.15.refs_1_), channel_id=1, source_target_pairs={{0,2},{1,3},{2,0},{3,1},{4,6},{5,7},{6,4},{7,5},{8,10},{9,11},{10,... | collective-permute-start | bytes 1179656 | tf_op jit(solution)/shard_map/ppermute | solution.py:43
  129.6 25.6 %collective-permute-start.35 = (bf16[384,512]{1,0:T(8,128)(2,1)S(1)}, bf16[384,512]{1,0:T(8,128)(2,1)S(1)}, u32[]{:S(2)}, u32[]{:S(2)}) collective-permute-start(bf16[384,512]{1,0:T(8,128)(2,1)S(1)} %bitcast.29), channel_id=1, source_target_pairs={{0,1},{1,0},{2,3},{3,2},{4,5},{5,4},{6,7},{7,6},{8,9},{9,8},{10,11... | collective-permute-start | bytes 1179656 | tf_op jit(solution)/shard_map/ppermute | solution.py:43
  135.6 26.5 %collective-permute-start.46 = (bf16[384,512]{1,0:T(8,128)(2,1)S(1)}, bf16[384,512]{1,0:T(8,128)(2,1)S(1)}, u32[]{:S(2)}, u32[]{:S(2)}) collective-permute-start(bf16[384,512]{1,0:T(8,128)(2,1)S(1)} %collective-permute-done.45.refs_2_), channel_id=1, source_target_pairs={{0,1},{1,0},{2,3},{3,2},{4,5},{5,4},{6,7},{7,6},{8,9},{9,8},{10,11... | collective-permute-start | bytes 1179656 | tf_op jit(solution)/shard_map/ppermute | solution.py:43
  137.8 27.5 %collective-permute-start.25 = (bf16[384,512]{1,0:T(8,128)(2,1)S(1)}, bf16[384,512]{1,0:T(8,128)(2,1)S(1)}, u32[]{:S(2)}, u32[]{:S(2)}) collective-permute-start(bf16[384,512]{1,0:T(8,128)(2,1)S(1)} %bitcast.36), channel_id=1, source_target_pairs={{0,1},{1,0},{2,3},{3,2},{4,5},{5,4},{6,7},{7,6},{8,9},{9,8},{10,11... | collective-permute-start | bytes 1179656 | tf_op jit(solution)/shard_map/ppermute | solution.py:43
  146.2 30.1 %collective-permute-start.36 = (bf16[384,512]{1,0:T(8,128)(2,1)S(1)}, bf16[384,512]{1,0:T(8,128)(2,1)S(1)}, u32[]{:S(2)}, u32[]{:S(2)}) collective-permute-start(bf16[384,512]{1,0:T(8,128)(2,1)S(1)} %bitcast.30), channel_id=1, source_target_pairs={{0,2},{1,3},{2,0},{3,1},{4,6},{5,7},{6,4},{7,5},{8,10},{9,11},{10,... | collective-permute-start | bytes 1179656 | tf_op jit(solution)/shard_map/ppermute | solution.py:43
  154.6 14.7 %collective-permute-start.27 = (bf16[384,512]{1,0:T(8,128)(2,1)S(1)}, bf16[384,512]{1,0:T(8,128)(2,1)S(1)}, u32[]{:S(2)}, u32[]{:S(2)}) collective-permute-start(bf16[384,512]{1,0:T(8,128)(2,1)S(1)} %collective-permute-done.26.refs_2_), channel_id=1, source_target_pairs={{0,1},{1,0},{2,3},{3,2},{4,5},{5,4},{6,7},{7,6},{8,9},{9,8},{10,11... | collective-permute-start | bytes 1179656 | tf_op jit(solution)/shard_map/ppermute | solution.py:43
  155.2 22.8 %collective-permute-start.37 = (bf16[384,512]{1,0:T(8,128)(2,1)S(1)}, bf16[384,512]{1,0:T(8,128)(2,1)S(1)}, u32[]{:S(2)}, u32[]{:S(2)}) collective-permute-start(bf16[384,512]{1,0:T(8,128)(2,1)S(1)} %collective-permute-done.35.refs_1_), channel_id=1, source_target_pairs={{0,2},{1,3},{2,0},{3,1},{4,6},{5,7},{6,4},{7,5},{8,10},{9,11},{10,... | collective-permute-start | bytes 1179656 | tf_op jit(solution)/shard_map/ppermute | solution.py:43
  162.2 13.5 %collective-permute-start.19 = (bf16[384,256]{1,0:T(8,128)(2,1)S(1)}, bf16[384,256]{1,0:T(8,128)(2,1)S(1)}, u32[]{:S(2)}, u32[]{:S(2)}) collective-permute-start(bf16[384,256]{1,0:T(8,128)(2,1)S(1)} %hidden_units.4.refs_0_), channel_id=1, source_target_pairs={{0,2},{1,3},{2,0},{3,1},{4,6},{5,7},{6,4},{7,5},{8,10},{9,11},{10,... | collective-permute-start | bytes 589832 | tf_op jit(solution)/shard_map/ppermute | solution.py:43
  165.4 15.7 %collective-permute-start.47 = (bf16[384,256]{1,0:T(8,128)(2,1)S(1)}, bf16[384,256]{1,0:T(8,128)(2,1)S(1)}, u32[]{:S(2)}, u32[]{:S(2)}) collective-permute-start(bf16[384,256]{1,0:T(8,128)(2,1)S(1)} %hidden_units.7.refs_0_), channel_id=1, source_target_pairs={{0,1},{1,0},{2,3},{3,2},{4,5},{5,4},{6,7},{7,6},{8,9},{9,8},{10,11... | collective-permute-start | bytes 589832 | tf_op jit(solution)/shard_map/ppermute | solution.py:43
  169.4 13.2 %collective-permute-start.48 = (bf16[384,256]{1,0:T(8,128)(2,1)S(1)}, bf16[384,256]{1,0:T(8,128)(2,1)S(1)}, u32[]{:S(2)}, u32[]{:S(2)}) collective-permute-start(bf16[384,256]{1,0:T(8,128)(2,1)S(1)} %hidden_units.7.refs_0_), channel_id=1, source_target_pairs={{0,2},{1,3},{2,0},{3,1},{4,6},{5,7},{6,4},{7,5},{8,10},{9,11},{10,... | collective-permute-start | bytes 589832 | tf_op jit(solution)/shard_map/ppermute | solution.py:43
  175.7 8.4 %collective-permute-start.29 = (bf16[384,256]{1,0:T(8,128)(2,1)S(1)}, bf16[384,256]{1,0:T(8,128)(2,1)S(1)}, u32[]{:S(2)}, u32[]{:S(2)}) collective-permute-start(bf16[384,256]{1,0:T(8,128)(2,1)S(1)} %hidden_units.5.refs_0_), channel_id=1, source_target_pairs={{0,2},{1,3},{2,0},{3,1},{4,6},{5,7},{6,4},{7,5},{8,10},{9,11},{10,... | collective-permute-start | bytes 589832 | tf_op jit(solution)/shard_map/ppermute | solution.py:43
  176.3 8.3 %collective-permute-start.18 = (bf16[384,256]{1,0:T(8,128)(2,1)S(1)}, bf16[384,256]{1,0:T(8,128)(2,1)S(1)}, u32[]{:S(2)}, u32[]{:S(2)}) collective-permute-start(bf16[384,256]{1,0:T(8,128)(2,1)S(1)} %hidden_units.4.refs_0_), channel_id=1, source_target_pairs={{0,1},{1,0},{2,3},{3,2},{4,5},{5,4},{6,7},{7,6},{8,9},{9,8},{10,11... | collective-permute-start | bytes 589832 | tf_op jit(solution)/shard_map/ppermute | solution.py:43
  178.0 10.3 %collective-permute-start.20 = (bf16[384,256]{1,0:T(8,128)(2,1)S(1)}, bf16[384,256]{1,0:T(8,128)(2,1)S(1)}, u32[]{:S(2)}, u32[]{:S(2)}) collective-permute-start(bf16[384,256]{1,0:T(8,128)(2,1)S(1)} %collective-permute-done.19.refs_2_), channel_id=1, source_target_pairs={{0,1},{1,0},{2,3},{3,2},{4,5},{5,4},{6,7},{7,6},{8,9},{9,8},{10,11... | collective-permute-start | bytes 589832 | tf_op jit(solution)/shard_map/ppermute | solution.py:43
  181.1 8.9 %collective-permute-start.39 = (bf16[384,256]{1,0:T(8,128)(2,1)S(1)}, bf16[384,256]{1,0:T(8,128)(2,1)S(1)}, u32[]{:S(2)}, u32[]{:S(2)}) collective-permute-start(bf16[384,256]{1,0:T(8,128)(2,1)S(1)} %hidden_units.6.refs_0_), channel_id=1, source_target_pairs={{0,2},{1,3},{2,0},{3,1},{4,6},{5,7},{6,4},{7,5},{8,10},{9,11},{10,... | collective-permute-start | bytes 589832 | tf_op jit(solution)/shard_map/ppermute | solution.py:43
  182.6 9.9 %collective-permute-start.28 = (bf16[384,256]{1,0:T(8,128)(2,1)S(1)}, bf16[384,256]{1,0:T(8,128)(2,1)S(1)}, u32[]{:S(2)}, u32[]{:S(2)}) collective-permute-start(bf16[384,256]{1,0:T(8,128)(2,1)S(1)} %hidden_units.5.refs_0_), channel_id=1, source_target_pairs={{0,1},{1,0},{2,3},{3,2},{4,5},{5,4},{6,7},{7,6},{8,9},{9,8},{10,11... | collective-permute-start | bytes 589832 | tf_op jit(solution)/shard_map/ppermute | solution.py:43
  184.1 12.6 %collective-permute-start.30 = (bf16[384,256]{1,0:T(8,128)(2,1)S(1)}, bf16[384,256]{1,0:T(8,128)(2,1)S(1)}, u32[]{:S(2)}, u32[]{:S(2)}) collective-permute-start(bf16[384,256]{1,0:T(8,128)(2,1)S(1)} %collective-permute-done.29.refs_2_), channel_id=1, source_target_pairs={{0,1},{1,0},{2,3},{3,2},{4,5},{5,4},{6,7},{7,6},{8,9},{9,8},{10,11... | collective-permute-start | bytes 589832 | tf_op jit(solution)/shard_map/ppermute | solution.py:43
  184.6 13.3 %collective-permute-start.49 = (bf16[384,256]{1,0:T(8,128)(2,1)S(1)}, bf16[384,256]{1,0:T(8,128)(2,1)S(1)}, u32[]{:S(2)}, u32[]{:S(2)}) collective-permute-start(bf16[384,256]{1,0:T(8,128)(2,1)S(1)} %collective-permute-done.47.refs_1_), channel_id=1, source_target_pairs={{0,2},{1,3},{2,0},{3,1},{4,6},{5,7},{6,4},{7,5},{8,10},{9,11},{10,... | collective-permute-start | bytes 589832 | tf_op jit(solution)/shard_map/ppermute | solution.py:43
  188.3 12.2 %collective-permute-start.38 = (bf16[384,256]{1,0:T(8,128)(2,1)S(1)}, bf16[384,256]{1,0:T(8,128)(2,1)S(1)}, u32[]{:S(2)}, u32[]{:S(2)}) collective-permute-start(bf16[384,256]{1,0:T(8,128)(2,1)S(1)} %hidden_units.6.refs_0_), channel_id=1, source_target_pairs={{0,1},{1,0},{2,3},{3,2},{4,5},{5,4},{6,7},{7,6},{8,9},{9,8},{10,11... | collective-permute-start | bytes 589832 | tf_op jit(solution)/shard_map/ppermute | solution.py:43
  190.0 13.5 %collective-permute-start.40 = (bf16[384,256]{1,0:T(8,128)(2,1)S(1)}, bf16[384,256]{1,0:T(8,128)(2,1)S(1)}, u32[]{:S(2)}, u32[]{:S(2)}) collective-permute-start(bf16[384,256]{1,0:T(8,128)(2,1)S(1)} %collective-permute-done.39.refs_2_), channel_id=1, source_target_pairs={{0,1},{1,0},{2,3},{3,2},{4,5},{5,4},{6,7},{7,6},{8,9},{9,8},{10,11... | collective-permute-start | bytes 589832 | tf_op jit(solution)/shard_map/ppermute | solution.py:43
  192.5 12.3 %collective-permute-start.21 = (bf16[192,512]{1,0:T(8,128)(2,1)S(1)}, bf16[192,512]{1,0:T(8,128)(2,1)S(1)}, u32[]{:S(2)}, u32[]{:S(2)}) collective-permute-start(bf16[192,512]{1,0:T(8,128)(2,1)S(1)} %get-tuple-element.41), channel_id=1, source_target_pairs={{0,24},{4,28},{8,0},{12,4},{16,8},{20,12},{24,16},{28,20},{1,25},{... | collective-permute-start | bytes 589832 | tf_op jit(solution)/shard_map/ppermute | solution.py:36
  196.7 8.9 %collective-permute-start.22 = (bf16[192,512]{1,0:T(8,128)(2,1)S(1)}, bf16[192,512]{1,0:T(8,128)(2,1)S(1)}, u32[]{:S(2)}, u32[]{:S(2)}) collective-permute-start(bf16[192,512]{1,0:T(8,128)(2,1)S(1)} %get-tuple-element.42), channel_id=1, source_target_pairs={{0,28},{4,24},{8,4},{12,0},{16,12},{20,8},{24,20},{28,16},{1,29},{... | collective-permute-start | bytes 589832 | tf_op jit(solution)/shard_map/ppermute | solution.py:36
  198.0 25.2 %collective-permute-start.31 = (bf16[192,512]{1,0:T(8,128)(2,1)S(1)}, bf16[192,512]{1,0:T(8,128)(2,1)S(1)}, u32[]{:S(2)}, u32[]{:S(2)}) collective-permute-start(bf16[192,512]{1,0:T(8,128)(2,1)S(1)} %get-tuple-element.43), channel_id=1, source_target_pairs={{0,16},{4,20},{8,24},{12,28},{16,0},{20,4},{24,8},{28,12},{1,17},{... | collective-permute-start | bytes 589832 | tf_op jit(solution)/shard_map/ppermute | solution.py:36
  200.5 26.9 %collective-permute-start.32 = (bf16[192,512]{1,0:T(8,128)(2,1)S(1)}, bf16[192,512]{1,0:T(8,128)(2,1)S(1)}, u32[]{:S(2)}, u32[]{:S(2)}) collective-permute-start(bf16[192,512]{1,0:T(8,128)(2,1)S(1)} %get-tuple-element.44), channel_id=1, source_target_pairs={{0,20},{4,16},{8,28},{12,24},{16,4},{20,0},{24,12},{28,8},{1,21},{... | collective-permute-start | bytes 589832 | tf_op jit(solution)/shard_map/ppermute | solution.py:36
  203.5 25.0 %collective-permute-start.50 = (bf16[192,512]{1,0:T(8,128)(2,1)S(1)}, bf16[192,512]{1,0:T(8,128)(2,1)S(1)}, u32[]{:S(2)}, u32[]{:S(2)}) collective-permute-start(bf16[192,512]{1,0:T(8,128)(2,1)S(1)} %get-tuple-element.50), channel_id=1, source_target_pairs={{0,4},{4,0},{8,12},{12,8},{16,20},{20,16},{24,28},{28,24},{1,5},{5... | collective-permute-start | bytes 589832 | tf_op jit(solution)/shard_map/ppermute | solution.py:36
  204.8 23.7 %collective-permute-start.41 = (bf16[192,512]{1,0:T(8,128)(2,1)S(1)}, bf16[192,512]{1,0:T(8,128)(2,1)S(1)}, u32[]{:S(2)}, u32[]{:S(2)}) collective-permute-start(bf16[192,512]{1,0:T(8,128)(2,1)S(1)} %get-tuple-element.47), channel_id=1, source_target_pairs={{0,8},{4,12},{8,16},{12,20},{16,24},{20,28},{24,0},{28,4},{1,9},{5... | collective-permute-start | bytes 589832 | tf_op jit(solution)/shard_map/ppermute | solution.py:36
  205.6 22.9 %collective-permute-start.42 = (bf16[192,512]{1,0:T(8,128)(2,1)S(1)}, bf16[192,512]{1,0:T(8,128)(2,1)S(1)}, u32[]{:S(2)}, u32[]{:S(2)}) collective-permute-start(bf16[192,512]{1,0:T(8,128)(2,1)S(1)} %get-tuple-element.48), channel_id=1, source_target_pairs={{0,12},{4,8},{8,20},{12,16},{16,28},{20,24},{24,4},{28,0},{1,13},{... | collective-permute-start | bytes 589832 | tf_op jit(solution)/shard_map/ppermute | solution.py:36
  (12 other events, 233.2 us)
where the time goes:
time: 231 us; the launch traced here: 230 us
  waiting for transfers between devices  120 us (52%)
  starting transfers between devices  57.4 us (25%)
  Pallas kernels  40.5 us (18%)
  local copies, waits for them, and re-layouts  7.9 us (3%)
  other arithmetic  3.47 us (2%)
    ppermute x27, waiting for transfers between devices, swap_tp(): return lax.ppermute(value, 'tp', [(i, i ^ mask) for i in range(count)])  58.4 us
    ppermute x13, waiting for transfers between devices, move_chips(): lax.ppermute(value, 'sp', [(i, (i + 2 * steps) % count ^ int(cross)) for...  54.6 us
    ppermute x27, starting transfers between devices, swap_tp(): return lax.ppermute(value, 'tp', [(i, i ^ mask) for i in range(count)])  28.7 us
    ppermute x13, starting transfers between devices, move_chips(): lax.ppermute(value, 'sp', [(i, (i + 2 * steps) % count ^ int(cross)) for...  14.1 us
    pallas_call x4, Pallas kernels, hidden_units(): pl.pallas_call(kernel, grid_spec=pltpu.PrefetchScalarGridSpec(num_scalar_...  10.9 us
    ppermute x3, starting transfers between devices, sent_states(): sent.append(lax.ppermute(chip, 'sp', pairs))  8.6 us
    pallas_call x1, Pallas kernels, mixer_project(): pl.pallas_call(kernel, grid_spec=pltpu.PrefetchScalarGridSpec(num_scalar_...  8.55 us
    pallas_call x1, Pallas kernels, mixer_local(): pl.pallas_call(kernel, grid=(groups,), in_specs=[pl.BlockSpec((length, st...  5.86 us
  transfers between devices with their start and end apart: 51, of which 26 were waited for; matrix products, arithmetic and copies ran while one was open for 1% of the time, Pallas kernels for 11%

commit v1 on v0

--- a/solution.py
+++ b/solution.py
@@ -428,18 +428,13 @@
     )(reads, halo, read_taps, values, writes, entering, cum)
 
 
-def mixer_project(local, reads, sums, arriving, gates, gain, weight, own, shares, groups):
+def mixer_mix(local, reads, sums, arriving, gates, gain, groups):
     heads, length = sums.shape
     channels, state = local.shape[1] // groups, reads.shape[1] // groups
     per_group = heads // groups
-    width = weight.shape[1] // shares
-
-    def kernel(own_ref, local_ref, read_ref, sum_ref, arrive_ref, gate_ref, gain_ref, *refs):
-        weights, outs = refs[:shares], refs[shares : 2 * shares]
-        mixed_ref, kept_ref = refs[2 * shares :]
+
+    def kernel(local_ref, read_ref, sum_ref, arrive_ref, gate_ref, gain_ref, out_ref):
         group = pl.program_id(0)
-        for m in range(shares):
-            kept_ref[m, pl.ds(pl.multiple_of(group * channels, channels), channels)] = weights[m][...]
         grown = to_channels(jnp.exp(sum_ref[...]), group, per_group, channels)
         y = local_ref[...] + grown * dot32(read_ref[...], arrive_ref[...])
         gated = y * silu(gate_ref[...].astype(jnp.float32))
@@ -447,37 +442,46 @@
         column = lax.broadcasted_iota(jnp.int32, (channels, channels), 1) // (channels // per_group)
         same = jnp.where(row == column, per_group / channels, 0.0).astype(jnp.bfloat16)
         mean = dot32((gated * gated).astype(jnp.bfloat16), same)
-        mixed_ref[group] = (gated * lax.rsqrt(mean + EPS) * gain_ref[...]).astype(jnp.bfloat16)
-
-        @pl.when(group == groups - 1)
-        def _():
-            mixed = jnp.concatenate([mixed_ref[g] for g in range(groups)], axis=1)
-            for m in reversed(range(shares)):
-                outs[m][...] = dot32(mixed, kept_ref[m]).astype(jnp.bfloat16)
-
-    by_group = lambda rows, width: pl.BlockSpec((rows, width), lambda g, o: (0, g))
-    whole = lambda rows, width: pl.BlockSpec((rows, width), lambda g, o: (0, 0))
-    share = lambda m: pl.BlockSpec((channels, width), lambda g, o: (g, o[0] ^ m))
+        out_ref[...] = (gated * lax.rsqrt(mean + EPS) * gain_ref[...]).astype(jnp.bfloat16)
+
+    by_group = lambda rows, width: pl.BlockSpec((rows, width), lambda g: (0, g))
+    return pl.pallas_call(
+        kernel,
+        grid=(groups,),
+        in_specs=[
+            by_group(length, channels), by_group(length, state),
+            pl.BlockSpec((heads, length), lambda g: (0, 0)),
+            by_group(state, channels), by_group(length, channels), by_group(1, channels),
+        ],
+        out_specs=by_group(length, channels),
+        out_shape=jax.ShapeDtypeStruct((length, groups * channels), jnp.bfloat16),
+        compiler_params=pltpu.CompilerParams(dimension_semantics=("arbitrary",), vmem_limit_bytes=VMEM_LIMIT),
+        name="mixer_mix",
+    )(local, reads, sums, arriving, gates, gain)
+
+
+def project_share(mixed, weight, own, mask, shares):
+    length, full = mixed.shape
+    width = weight.shape[1] // shares
+
+    def kernel(own_ref, mixed_ref, weight_ref, out_ref):
+        out_ref[...] = dot32(mixed_ref[...], weight_ref[...]).astype(jnp.bfloat16)
+
     return pl.pallas_call(
         kernel,
         grid_spec=pltpu.PrefetchScalarGridSpec(
             num_scalar_prefetch=1,
-            grid=(groups,),
+            grid=(1,),
             in_specs=[
-                by_group(length, channels), by_group(length, state), whole(heads, length),
-                by_group(state, channels), by_group(length, channels), by_group(1, channels),
-            ]
-            + [share(m) for m in range(shares)],
-            out_specs=[whole(length, width) for _ in range(shares)],
-            scratch_shapes=[
-                pltpu.VMEM((groups, length, channels), jnp.bfloat16),
-                pltpu.VMEM((shares, weight.shape[0], width), jnp.bfloat16),
+                pl.BlockSpec((length, full), lambda i, o: (0, 0)),
+                pl.BlockSpec((full, width), lambda i, o: (0, o[0] ^ mask)),
             ],
-        ),
-        out_shape=[jax.ShapeDtypeStruct((length, width), jnp.bfloat16) for _ in range(shares)],
-        compiler_params=pltpu.CompilerParams(dimension_semantics=("arbitrary",), vmem_limit_bytes=MIXER_LIMIT),
-        name="mixer_project",
-    )(own, local, reads, sums, arriving, gates, gain, *[weight] * shares)
+            out_specs=pl.BlockSpec((length, width), lambda i, o: (0, 0)),
+        ),
+        out_shape=jax.ShapeDtypeStruct((length, width), jnp.bfloat16),
+        compiler_params=pltpu.CompilerParams(vmem_limit_bytes=VMEM_LIMIT),
+        name="project_share",
+    )(own, mixed, weight)
 
 
 def sent_states(closing, state):
@@ -594,22 +598,16 @@
     inverse = jnp.broadcast_to((1.0 / (ffn_gain * ffn_gain))[:, None], (ffn_gain.shape[0], 128))
     inverse = inverse.astype(jnp.bfloat16)
     arriving = arriving_state(sent, other, state_dim)
-    leaving = mixer_project(
-        local,
-        reads,
-        sums,
-        arriving,
-        gate_act,
-        inner_gain[None],
-        out_weight,
-        own_index,
-        tp_count,
-        groups_here,
-    )
-    projected = leaving[0].astype(jnp.float32)
-    for m in reversed(range(1, tp_count)):
-        part = swap_tp(leaving[m], m)
-        projected = projected + part.astype(jnp.float32)
+    mixed = mixer_mix(local, reads, sums, arriving, gate_act, inner_gain[None], groups_here)
+    partials = []
+    for m in reversed(range(tp_count)):
+        share = project_share(mixed, out_weight, own_index, m, tp_count)
+        if m:
+            share = swap_tp(share, m)
+        partials.append(share.astype(jnp.float32))
+    projected = partials[-1]
+    for part in partials[:-1]:
+        projected = projected + part
     kept = share_of.astype(jnp.float32) + projected
     rows = (kept * gain_share[None, :]).astype(jnp.bfloat16)
     blocks_of = []

time: 231 us -> 229 us (level)
  local copies, waits for them, and re-layouts: 7.9 us -> 12.6 us
  Pallas kernels: 40.5 us -> 37.4 us
  waiting for transfers between devices: 120 us -> 117 us
    unnamed x19 -> x33, local copies, waits for them, and re-layouts: 4.16 us -> 8.9 us
    pallas_call x1 -> x5, Pallas kernels: 8.55 us -> 5.25 us  [the longest x1 2.94 us: mixer_mix(): pl.pallas_call(kernel, grid=(groups,), in_specs=[by_group(length, channel...]
    ppermute x27, waiting for transfers between devices: 58.4 us -> 55.3 us  [swap_tp(): return lax.ppermute(value, 'tp', [(i, i ^ mask) for i in range(count)])]
where the time goes in v1:
time: 229 us; the launch traced here: 228 us
  waiting for transfers between devices  117 us (51%)
  starting transfers between devices  57.4 us (25%)
  Pallas kernels  37.4 us (16%)
  local copies, waits for them, and re-layouts  12.6 us (6%)
  other arithmetic  2.63 us (1%)
    ppermute x27, waiting for transfers between devices, swap_tp(): return lax.ppermute(value, 'tp', [(i, i ^ mask) for i in range(count)])  55.3 us
    ppermute x13, waiting for transfers between devices, move_chips(): lax.ppermute(value, 'sp', [(i, (i + 2 * steps) % count ^ int(cross)) for...  54.7 us
    ppermute x27, starting transfers between devices, swap_tp(): return lax.ppermute(value, 'tp', [(i, i ^ mask) for i in range(count)])  28.7 us
    ppermute x13, starting transfers between devices, move_chips(): lax.ppermute(value, 'sp', [(i, (i + 2 * steps) % count ^ int(cross)) for...  14.1 us
    pallas_call x4, Pallas kernels, hidden_units(): pl.pallas_call(kernel, grid_spec=pltpu.PrefetchScalarGridSpec(num_scalar_...  11 us
    unnamed x33, local copies, waits for them, and re-layouts  8.9 us
    ppermute x3, starting transfers between devices, sent_states(): sent.append(lax.ppermute(chip, 'sp', pairs))  8.62 us
    pallas_call x1, Pallas kernels, mixer_local(): pl.pallas_call(kernel, grid=(groups,), in_specs=[pl.BlockSpec((length, st...  5.91 us
  transfers between devices with their start and end apart: 51, of which 26 were waited for; matrix products, arithmetic and copies ran while one was open for 1% of the time, Pallas kernels for 11%

profile of v1, /device:TPU:0, one launch (start us, length us, event | category | flops | bytes accessed | tf_op | source)
XLA Modules:
  0.0 228.2 jit_solution(3789281926790285239)
XLA Ops:
  2.2 2.4 %collective-permute-start = (bf16[16,2048]{1,0:T(8,128)(2,1)S(1)}, bf16[16,2048]{1,0:T(8,128)(2,1)S(1)}, u32[]{:S(2)}, u32[]{:S(2)}) collective-permute-start(bf16[16,2048]{1,0:T(8,128)(2,1)S(1)} %pad_maximum_fusion.1), channel_id=1, source_target_pairs={{0,4},{4,8},{8,12},{12,16},{16,20},{20,24},{24,28},{1,5},{5,9},{9,... | collective-permute-start | bytes 196616 | tf_op jit(solution)/shard_map/ppermute | solution.py:22
  7.7 5.8 %mixer_states.1 = (bf16[384,1024]{1,0:T(8,128)(2,1)}, bf16[384,512]{1,0:T(8,128)(2,1)}, f32[16,384]{1,0:T(8,128)}, f32[16,384]{1,0:T(8,128)}, bf16[384,1024]{1,0:T(8,128)(2,1)}, /*index=5*/bf16[144,1024]{1,0:T(8,128)(2,1)}) custom-call(bf16[384,1024]{1,0:T(8,128)(2,1)} %act_ref.1, bf16[384,1024]{1,0:T(8,128)(2,1)} %copy-done.12, ...), custom_call_target="tpu_custom_call" | custom-call | tf_op jit(solution)/shard_map/mixer_states/pallas_call | solution.py:347
  13.4 2.7 %collective-permute-start.1 = (bf16[144,1024]{1,0:T(8,128)(2,1)}, bf16[144,1024]{1,0:T(8,128)(2,1)S(1)}, u32[]{:S(2)}, u32[]{:S(2)}) collective-permute-start(bf16[144,1024]{1,0:T(8,128)(2,1)} %get-tuple-element.31), channel_id=1, source_target_pairs={{0,4},{4,0},{8,12},{12,8},{16,20},{20,16},{24,28},{28,24},{1,5},{5... | collective-permute-start | bytes 884744 | tf_op jit(solution)/shard_map/ppermute | solution.py:31
  18.7 3.5 %collective-permute-start.2 = (bf16[144,512]{1,0:T(8,128)(2,1)S(1)}, bf16[144,512]{1,0:T(8,128)(2,1)S(1)}, u32[]{:S(2)}, u32[]{:S(2)}) collective-permute-start(bf16[144,512]{1,0:T(8,128)(2,1)S(1)} %pad_maximum_fusion), channel_id=1, source_target_pairs={{0,8},{4,12},{8,16},{12,20},{16,24},{20,28},{1,9},{5,13},{9,17},{1... | collective-permute-start | bytes 442376 | tf_op jit(solution)/shard_map/ppermute | solution.py:502
  22.2 3.3 %collective-permute-start.4 = (bf16[144,512]{1,0:T(8,128)(2,1)S(1)}, bf16[144,512]{1,0:T(8,128)(2,1)S(1)}, u32[]{:S(2)}, u32[]{:S(2)}) collective-permute-start(bf16[144,512]{1,0:T(8,128)(2,1)S(1)} %pad_maximum_fusion), channel_id=1, source_target_pairs={{0,24},{4,28},{1,25},{5,29},{2,26},{6,30},{3,27},{7,31}} | collective-permute-start | bytes 442376 | tf_op jit(solution)/shard_map/ppermute | solution.py:502
  25.5 1.9 collective-permute-start.3
  27.4 2.3 %collective-permute-done.4 = bf16[144,512]{1,0:T(8,128)(2,1)S(1)} collective-permute-done((bf16[144,512]{1,0:T(8,128)(2,1)S(1)}, bf16[144,512]{1,0:T(8,128)(2,1)S(1)}, u32[]{:S(2)}, u32[]{:S(2)}) %collective-permute-start.4) | collective-permute-done | bytes 147488 | tf_op jit(solution)/shard_map/ppermute | solution.py:502
  29.8 2.4 %collective-permute-done.3 = bf16[144,512]{1,0:T(8,128)(2,1)S(1)} collective-permute-done((bf16[144,512]{1,0:T(8,128)(2,1)S(1)}, bf16[144,512]{1,0:T(8,128)(2,1)S(1)}, u32[]{:S(2)}, u32[]{:S(2)}) %collective-permute-start.3) | collective-permute-done | bytes 147488 | tf_op jit(solution)/shard_map/ppermute | solution.py:502
  32.4 5.9 %mixer_local.1 = (f32[384,1024]{1,0:T(8,128)}, bf16[384,512]{1,0:T(8,128)(2,1)}) custom-call(bf16[384,1024]{1,0:T(8,128)(2,1)} %copy-done.12, bf16[16,2048]{1,0:T(8,128)(2,1)} %copy-done.13, bf16[4,4,128]{2,1,0:T(4,128)(2,1)} %taps_ref.3, bf16[384,1024]{1,0:T(8,128)(2,1)} %get-tuple-element.24.value_ref, bf16[384,512]{1,0:T(8,128)(2,1)} %get-tuple-element.25.write_ref, ...), custom_call_target="tpu_custom_call" | custom-call | flops 4000000000 | bytes 4000000 | tf_op jit(solution)/shard_map/mixer_local/pallas_call | solution.py:408
  41.1 2.9 %mixer_mix.1.mixed_ref = bf16[384,1024]{1,0:T(8,128)(2,1)S(1)} custom-call(f32[384,1024]{1,0:T(8,128)S(1)} %copy-done.6, bf16[384,512]{1,0:T(8,128)(2,1)S(1)} %copy-done.8, f32[16,384]{1,0:T(8,128)S(1)} %copy-done.9, bf16[128,1024]{1,0:T(8,128)(2,1)S(1)} %fusion.1.arrive_ref, bf16[384,1024]{1,0:T(8,128)(2,1)S(1)} %copy-done.7, f32[1,1024]{1,0:T(1,128)S(1)} %bitcast.41), custom_call_target="tpu_custom_call" | custom-call | tf_op jit(solution)/shard_map/mixer_mix/pallas_call | solution.py:448
  45.8 2.5 %collective-permute-start.6 = (bf16[384,512]{1,0:T(8,128)(2,1)S(1)}, bf16[384,512]{1,0:T(8,128)(2,1)S(1)}, u32[]{:S(2)}, u32[]{:S(2)}) collective-permute-start(bf16[384,512]{1,0:T(8,128)(2,1)S(1)} %project_share.5), channel_id=1, source_target_pairs={{0,3},{1,2},{2,1},{3,0},{4,7},{5,6},{6,5},{7,4},{8,11},{9,10},{10,... | collective-permute-start | bytes 1179656 | tf_op jit(solution)/shard_map/ppermute | solution.py:43
  49.5 2.2 copy-done.2
  52.2 6.6 %collective-permute-done.6 = bf16[384,512]{1,0:T(8,128)(2,1)S(1)} collective-permute-done((bf16[384,512]{1,0:T(8,128)(2,1)S(1)}, bf16[384,512]{1,0:T(8,128)(2,1)S(1)}, u32[]{:S(2)}, u32[]{:S(2)}) %collective-permute-start.6) | collective-permute-done | bytes 393248 | tf_op jit(solution)/shard_map/ppermute | solution.py:43
  58.8 7.9 %collective-permute-done.7 = bf16[384,512]{1,0:T(8,128)(2,1)S(1)} collective-permute-done((bf16[384,512]{1,0:T(8,128)(2,1)S(1)}, bf16[384,512]{1,0:T(8,128)(2,1)S(1)}, u32[]{:S(2)}, u32[]{:S(2)}) %collective-permute-start.7) | collective-permute-done | bytes 393248 | tf_op jit(solution)/shard_map/ppermute | solution.py:43
  68.1 4.7 %collective-permute-start.9 = (bf16[384,512]{1,0:T(8,128)(2,1)S(1)}, bf16[384,512]{1,0:T(8,128)(2,1)S(1)}, u32[]{:S(2)}, u32[]{:S(2)}) collective-permute-start(bf16[384,512]{1,0:T(8,128)(2,1)S(1)} %get-tuple-element.43.refs_0_), channel_id=1, source_target_pairs={{0,8},{4,12},{8,16},{12,20},{16,24},{20,28},{24,0},{28,4},{1,9},{5... | collective-permute-start | bytes 1179656 | tf_op jit(solution)/shard_map/ppermute | solution.py:36
  72.8 12.0 %collective-permute-done.9.refs_0_ = bf16[384,512]{1,0:T(8,128)(2,1)S(1)} collective-permute-done((bf16[384,512]{1,0:T(8,128)(2,1)S(1)}, bf16[384,512]{1,0:T(8,128)(2,1)S(1)}, u32[]{:S(2)}, u32[]{:S(2)}) %collective-permute-start.9) | collective-permute-done | bytes 393248 | tf_op jit(solution)/shard_map/ppermute | solution.py:36
  84.9 12.2 %collective-permute-done.23.refs_0_ = bf16[384,512]{1,0:T(8,128)(2,1)S(1)} collective-permute-done((bf16[384,512]{1,0:T(8,128)(2,1)S(1)}, bf16[384,512]{1,0:T(8,128)(2,1)S(1)}, u32[]{:S(2)}, u32[]{:S(2)}) %collective-permute-start.23) | collective-permute-done | bytes 393248 | tf_op jit(solution)/shard_map/ppermute | solution.py:36
  98.8 4.4 %collective-permute-start.13 = (s32[4,384]{1,0:T(4,128)S(1)}, s32[4,384]{1,0:T(4,128)S(1)}, u32[]{:S(2)}, u32[]{:S(2)}) collective-permute-start(s32[4,384]{1,0:T(4,128)S(1)} %pad_add_fusion), channel_id=1, source_target_pairs={{0,16},{4,20},{8,24},{12,28},{16,0},{20,4},{24,8},{28,12},{1,17},{... | collective-permute-start | bytes 18440 | tf_op jit(solution)/shard_map/ppermute | solution.py:36
  103.2 5.5 %collective-permute-done.12 = s32[4,384]{1,0:T(4,128)S(1)} collective-permute-done((s32[4,384]{1,0:T(4,128)S(1)}, s32[4,384]{1,0:T(4,128)S(1)}, u32[]{:S(2)}, u32[]{:S(2)}) %collective-permute-start.12) | collective-permute-done | bytes 6176 | tf_op jit(solution)/shard_map/ppermute | solution.py:36
  108.8 3.5 %collective-permute-done.14 = s32[4,384]{1,0:T(4,128)S(1)} collective-permute-done((s32[4,384]{1,0:T(4,128)S(1)}, s32[4,384]{1,0:T(4,128)S(1)}, u32[]{:S(2)}, u32[]{:S(2)}) %collective-permute-start.14) | collective-permute-done | bytes 6176 | tf_op jit(solution)/shard_map/ppermute | solution.py:36
  113.0 1.6 collective-permute-start.15
  115.8 1.7 collective-permute-start.44
  118.2 6.9 %collective-permute-done.15.refs_1_ = bf16[384,512]{1,0:T(8,128)(2,1)S(1)} collective-permute-done((bf16[384,512]{1,0:T(8,128)(2,1)S(1)}, bf16[384,512]{1,0:T(8,128)(2,1)S(1)}, u32[]{:S(2)}, u32[]{:S(2)}) %collective-permute-start.15) | collective-permute-done | bytes 393248 | tf_op jit(solution)/shard_map/ppermute | solution.py:43
  125.1 1.7 collective-permute-start.26
  129.0 4.5 %collective-permute-done.44.refs_1_ = bf16[384,512]{1,0:T(8,128)(2,1)S(1)} collective-permute-done((bf16[384,512]{1,0:T(8,128)(2,1)S(1)}, bf16[384,512]{1,0:T(8,128)(2,1)S(1)}, u32[]{:S(2)}, u32[]{:S(2)}) %collective-permute-start.44) | collective-permute-done | bytes 393248 | tf_op jit(solution)/shard_map/ppermute | solution.py:43
  136.2 7.9 %collective-permute-done.26.refs_2_ = bf16[384,512]{1,0:T(8,128)(2,1)S(1)} collective-permute-done((bf16[384,512]{1,0:T(8,128)(2,1)S(1)}, bf16[384,512]{1,0:T(8,128)(2,1)S(1)}, u32[]{:S(2)}, u32[]{:S(2)}) %collective-permute-start.26) | collective-permute-done | bytes 393248 | tf_op jit(solution)/shard_map/ppermute | solution.py:43
  144.7 7.8 %collective-permute-done.17.refs_3_ = bf16[384,512]{1,0:T(8,128)(2,1)S(1)} collective-permute-done((bf16[384,512]{1,0:T(8,128)(2,1)S(1)}, bf16[384,512]{1,0:T(8,128)(2,1)S(1)}, u32[]{:S(2)}, u32[]{:S(2)}) %collective-permute-start.17) | collective-permute-done | bytes 393248 | tf_op jit(solution)/shard_map/ppermute | solution.py:43
  153.0 1.7 collective-permute-start.37
  155.1 2.2 copy-done.4
  157.3 2.7 %hidden_units.4.refs_0_ = bf16[384,256]{1,0:T(8,128)(2,1)S(1)} custom-call(s32[1]{0:T(128)} %bitcast.own_ref, bf16[384,512]{1,0:T(8,128)(2,1)S(1)} %bitcast.34, bf16[384,512]{1,0:T(8,128)(2,1)S(1)} %collective-permute-done.15.refs_1_, bf16[384,512]{1,0:T(8,128)(2,1)S(1)} %collective-permute-done.16.refs_2_, ...), custom_call_target="tpu_custom_call" | custom-call | flops 805306368 | bytes 8388608 | tf_op jit(solution)/shard_map/hidden_units/pallas_call | solution.py:151
  160.4 2.8 %hidden_units.7.refs_0_ = bf16[384,256]{1,0:T(8,128)(2,1)S(1)} custom-call(s32[1]{0:T(128)} %bitcast.own_ref, bf16[384,512]{1,0:T(8,128)(2,1)S(1)} %bitcast.40, bf16[384,512]{1,0:T(8,128)(2,1)S(1)} %collective-permute-done.44.refs_1_, bf16[384,512]{1,0:T(8,128)(2,1)S(1)} %collective-permute-done.45.refs_2_, ...), custom_call_target="tpu_custom_call" | custom-call | flops 805306368 | bytes 8388608 | tf_op jit(solution)/shard_map/hidden_units/pallas_call | solution.py:151
  163.2 1.6 collective-permute-start.47
  164.8 2.4 %collective-permute-done.27.refs_3_ = bf16[384,512]{1,0:T(8,128)(2,1)S(1)} collective-permute-done((bf16[384,512]{1,0:T(8,128)(2,1)S(1)}, bf16[384,512]{1,0:T(8,128)(2,1)S(1)}, u32[]{:S(2)}, u32[]{:S(2)}) %collective-permute-start.27) | collective-permute-done | bytes 393248 | tf_op jit(solution)/shard_map/ppermute | solution.py:43
  167.2 1.7 collective-permute-start.48
  168.9 2.7 %hidden_units.5.refs_0_ = bf16[384,256]{1,0:T(8,128)(2,1)S(1)} custom-call(s32[1]{0:T(128)} %bitcast.own_ref, bf16[384,512]{1,0:T(8,128)(2,1)S(1)} %bitcast.37, bf16[384,512]{1,0:T(8,128)(2,1)S(1)} %collective-permute-done.25.refs_1_, bf16[384,512]{1,0:T(8,128)(2,1)S(1)} %collective-permute-done.26.refs_2_, ...), custom_call_target="tpu_custom_call" | custom-call | flops 805306368 | bytes 8388608 | tf_op jit(solution)/shard_map/hidden_units/pallas_call | solution.py:151
  171.7 1.9 collective-permute-done.19.refs_2_
  174.2 1.7 collective-permute-start.18
  176.2 2.8 %hidden_units.6.refs_0_ = bf16[384,256]{1,0:T(8,128)(2,1)S(1)} custom-call(s32[1]{0:T(128)} %bitcast.own_ref, bf16[384,512]{1,0:T(8,128)(2,1)S(1)} %bitcast.31, bf16[384,512]{1,0:T(8,128)(2,1)S(1)} %collective-permute-done.35.refs_1_, bf16[384,512]{1,0:T(8,128)(2,1)S(1)} %collective-permute-done.36.refs_2_, ...), custom_call_target="tpu_custom_call" | custom-call | flops 805306368 | bytes 8388608 | tf_op jit(solution)/shard_map/hidden_units/pallas_call | solution.py:151
  182.5 1.7 collective-permute-start.49
  184.3 1.9 collective-permute-done.20.refs_3_
  186.2 1.7 collective-permute-start.38
  190.4 1.8 collective-permute-start.21
  192.2 2.4 %collective-permute-done.30.refs_3_ = bf16[384,256]{1,0:T(8,128)(2,1)S(1)} collective-permute-done((bf16[384,256]{1,0:T(8,128)(2,1)S(1)}, bf16[384,256]{1,0:T(8,128)(2,1)S(1)}, u32[]{:S(2)}, u32[]{:S(2)}) %collective-permute-start.30) | collective-permute-done | bytes 196640 | tf_op jit(solution)/shard_map/ppermute | solution.py:43
  195.9 2.4 %collective-permute-done.38.refs_1_ = bf16[384,256]{1,0:T(8,128)(2,1)S(1)} collective-permute-done((bf16[384,256]{1,0:T(8,128)(2,1)S(1)}, bf16[384,256]{1,0:T(8,128)(2,1)S(1)}, u32[]{:S(2)}, u32[]{:S(2)}) %collective-permute-start.38) | collective-permute-done | bytes 196640 | tf_op jit(solution)/shard_map/ppermute | solution.py:43
  198.3 1.7 collective-permute-start.32
  203.9 17.1 %collective-permute-done.31.refs_2_ = bf16[192,512]{1,0:T(8,128)(2,1)S(1)} collective-permute-done((bf16[192,512]{1,0:T(8,128)(2,1)S(1)}, bf16[192,512]{1,0:T(8,128)(2,1)S(1)}, u32[]{:S(2)}, u32[]{:S(2)}) %collective-permute-start.31) | collective-permute-done | bytes 196640 | tf_op jit(solution)/shard_map/ppermute | solution.py:36
  221.0 4.3 %collective-permute-done.32.refs_3_ = bf16[192,512]{1,0:T(8,128)(2,1)S(1)} collective-permute-done((bf16[192,512]{1,0:T(8,128)(2,1)S(1)}, bf16[192,512]{1,0:T(8,128)(2,1)S(1)}, u32[]{:S(2)}, u32[]{:S(2)}) %collective-permute-start.32) | collective-permute-done | bytes 196640 | tf_op jit(solution)/shard_map/ppermute | solution.py:36
  226.4 1.8 combine.3
  (137 shorter events, 39.9 us)
Async XLA Ops:
  2.2 4.5 %collective-permute-start = (bf16[16,2048]{1,0:T(8,128)(2,1)S(1)}, bf16[16,2048]{1,0:T(8,128)(2,1)S(1)}, u32[]{:S(2)}, u32[]{:S(2)}) collective-permute-start(bf16[16,2048]{1,0:T(8,128)(2,1)S(1)} %pad_maximum_fusion.1), channel_id=1, source_target_pairs={{0,4},{4,8},{8,12},{12,16},{16,20},{20,24},{24,28},{1,5},{5,9},{9,... | collective-permute-start | bytes 196616 | tf_op jit(solution)/shard_map/ppermute | solution.py:22
  18.7 8.6 %collective-permute-start.2 = (bf16[144,512]{1,0:T(8,128)(2,1)S(1)}, bf16[144,512]{1,0:T(8,128)(2,1)S(1)}, u32[]{:S(2)}, u32[]{:S(2)}) collective-permute-start(bf16[144,512]{1,0:T(8,128)(2,1)S(1)} %pad_maximum_fusion), channel_id=1, source_target_pairs={{0,8},{4,12},{8,16},{12,20},{16,24},{20,28},{1,9},{5,13},{9,17},{1... | collective-permute-start | bytes 442376 | tf_op jit(solution)/shard_map/ppermute | solution.py:502
  22.2 7.5 %collective-permute-start.4 = (bf16[144,512]{1,0:T(8,128)(2,1)S(1)}, bf16[144,512]{1,0:T(8,128)(2,1)S(1)}, u32[]{:S(2)}, u32[]{:S(2)}) collective-permute-start(bf16[144,512]{1,0:T(8,128)(2,1)S(1)} %pad_maximum_fusion), channel_id=1, source_target_pairs={{0,24},{4,28},{1,25},{5,29},{2,26},{6,30},{3,27},{7,31}} | collective-permute-start | bytes 442376 | tf_op jit(solution)/shard_map/ppermute | solution.py:502
  25.5 6.7 %collective-permute-start.3 = (bf16[144,512]{1,0:T(8,128)(2,1)S(1)}, bf16[144,512]{1,0:T(8,128)(2,1)S(1)}, u32[]{:S(2)}, u32[]{:S(2)}) collective-permute-start(bf16[144,512]{1,0:T(8,128)(2,1)S(1)} %pad_maximum_fusion), channel_id=1, source_target_pairs={{0,16},{4,20},{8,24},{12,28},{1,17},{5,21},{9,25},{13,29},{2,18},{... | collective-permute-start | bytes 442376 | tf_op jit(solution)/shard_map/ppermute | solution.py:502
  32.3 6.1 %collective-permute-start.5 = (bf16[128,512]{1,0:T(8,128)(2,1)S(1)}, bf16[128,512]{1,0:T(8,128)(2,1)S(1)}, u32[]{:S(2)}, u32[]{:S(2)}) collective-permute-start(bf16[128,512]{1,0:T(8,128)(2,1)S(1)} %fusion.6), channel_id=1, source_target_pairs={{0,4},{4,0},{8,12},{12,8},{16,20},{20,16},{24,28},{28,24},{1,5},{5... | collective-permute-start | bytes 393224 | tf_op jit(solution)/shard_map/ppermute | solution.py:31
  45.8 13.0 %collective-permute-start.6 = (bf16[384,512]{1,0:T(8,128)(2,1)S(1)}, bf16[384,512]{1,0:T(8,128)(2,1)S(1)}, u32[]{:S(2)}, u32[]{:S(2)}) collective-permute-start(bf16[384,512]{1,0:T(8,128)(2,1)S(1)} %project_share.5), channel_id=1, source_target_pairs={{0,3},{1,2},{2,1},{3,0},{4,7},{5,6},{6,5},{7,4},{8,11},{9,10},{10,... | collective-permute-start | bytes 1179656 | tf_op jit(solution)/shard_map/ppermute | solution.py:43
  48.4 18.4 %collective-permute-start.7 = (bf16[384,512]{1,0:T(8,128)(2,1)S(1)}, bf16[384,512]{1,0:T(8,128)(2,1)S(1)}, u32[]{:S(2)}, u32[]{:S(2)}) collective-permute-start(bf16[384,512]{1,0:T(8,128)(2,1)S(1)} %project_share.6), channel_id=1, source_target_pairs={{0,2},{1,3},{2,0},{3,1},{4,6},{5,7},{6,4},{7,5},{8,10},{9,11},{10,... | collective-permute-start | bytes 1179656 | tf_op jit(solution)/shard_map/ppermute | solution.py:43
  48.9 17.9 %collective-permute-start.8 = (bf16[384,512]{1,0:T(8,128)(2,1)S(1)}, bf16[384,512]{1,0:T(8,128)(2,1)S(1)}, u32[]{:S(2)}, u32[]{:S(2)}) collective-permute-start(bf16[384,512]{1,0:T(8,128)(2,1)S(1)} %project_share.7), channel_id=1, source_target_pairs={{0,1},{1,0},{2,3},{3,2},{4,5},{5,4},{6,7},{7,6},{8,9},{9,8},{10,11... | collective-permute-start | bytes 1179656 | tf_op jit(solution)/shard_map/ppermute | solution.py:43
  68.1 16.8 %collective-permute-start.9 = (bf16[384,512]{1,0:T(8,128)(2,1)S(1)}, bf16[384,512]{1,0:T(8,128)(2,1)S(1)}, u32[]{:S(2)}, u32[]{:S(2)}) collective-permute-start(bf16[384,512]{1,0:T(8,128)(2,1)S(1)} %get-tuple-element.43.refs_0_), channel_id=1, source_target_pairs={{0,8},{4,12},{8,16},{12,20},{16,24},{20,28},{24,0},{28,4},{1,9},{5... | collective-permute-start | bytes 1179656 | tf_op jit(solution)/shard_map/ppermute | solution.py:36
  84.9 12.2 %collective-permute-start.23 = (bf16[384,512]{1,0:T(8,128)(2,1)S(1)}, bf16[384,512]{1,0:T(8,128)(2,1)S(1)}, u32[]{:S(2)}, u32[]{:S(2)}) collective-permute-start(bf16[384,512]{1,0:T(8,128)(2,1)S(1)} %collective-permute-done.9.refs_0_), channel_id=1, source_target_pairs={{0,8},{4,12},{8,16},{12,20},{16,24},{20,28},{24,0},{28,4},{1,9},{5... | collective-permute-start | bytes 1179656 | tf_op jit(solution)/shard_map/ppermute | solution.py:36
  84.9 27.8 %collective-permute-start.10 = (bf16[384,512]{1,0:T(8,128)(2,1)S(1)}, bf16[384,512]{1,0:T(8,128)(2,1)S(1)}, u32[]{:S(2)}, u32[]{:S(2)}) collective-permute-start(bf16[384,512]{1,0:T(8,128)(2,1)S(1)} %collective-permute-done.9.refs_0_), channel_id=1, source_target_pairs={{0,4},{4,0},{8,12},{12,8},{16,20},{20,16},{24,28},{28,24},{1,5},{5... | collective-permute-start | bytes 1179656 | tf_op jit(solution)/shard_map/ppermute | solution.py:31
  97.0 17.6 %collective-permute-start.33 = (bf16[384,512]{1,0:T(8,128)(2,1)S(1)}, bf16[384,512]{1,0:T(8,128)(2,1)S(1)}, u32[]{:S(2)}, u32[]{:S(2)}) collective-permute-start(bf16[384,512]{1,0:T(8,128)(2,1)S(1)} %collective-permute-done.23.refs_0_), channel_id=1, source_target_pairs={{0,8},{4,12},{8,16},{12,20},{16,24},{20,28},{24,0},{28,4},{1,9},{5... | collective-permute-start | bytes 1179656 | tf_op jit(solution)/shard_map/ppermute | solution.py:36
  97.0 17.8 %collective-permute-start.43 = (bf16[384,512]{1,0:T(8,128)(2,1)S(1)}, bf16[384,512]{1,0:T(8,128)(2,1)S(1)}, u32[]{:S(2)}, u32[]{:S(2)}) collective-permute-start(bf16[384,512]{1,0:T(8,128)(2,1)S(1)} %get-tuple-element.43.refs_0_), channel_id=1, source_target_pairs={{0,4},{4,0},{8,12},{12,8},{16,20},{20,16},{24,28},{28,24},{1,5},{5... | collective-permute-start | bytes 1179656 | tf_op jit(solution)/shard_map/ppermute | solution.py:31
  98.8 9.9 %collective-permute-start.12 = (s32[4,384]{1,0:T(4,128)S(1)}, s32[4,384]{1,0:T(4,128)S(1)}, u32[]{:S(2)}, u32[]{:S(2)}) collective-permute-start(s32[4,384]{1,0:T(4,128)S(1)} %pad_add_fusion), channel_id=1, source_target_pairs={{0,8},{4,12},{8,16},{12,20},{16,24},{20,28},{24,0},{28,4},{1,9},{5... | collective-permute-start | bytes 18440 | tf_op jit(solution)/shard_map/ppermute | solution.py:36
  98.8 9.9 %collective-permute-start.13 = (s32[4,384]{1,0:T(4,128)S(1)}, s32[4,384]{1,0:T(4,128)S(1)}, u32[]{:S(2)}, u32[]{:S(2)}) collective-permute-start(s32[4,384]{1,0:T(4,128)S(1)} %pad_add_fusion), channel_id=1, source_target_pairs={{0,16},{4,20},{8,24},{12,28},{16,0},{20,4},{24,8},{28,12},{1,17},{... | collective-permute-start | bytes 18440 | tf_op jit(solution)/shard_map/ppermute | solution.py:36
  112.6 4.9 %collective-permute-start.24 = (bf16[384,512]{1,0:T(8,128)(2,1)S(1)}, bf16[384,512]{1,0:T(8,128)(2,1)S(1)}, u32[]{:S(2)}, u32[]{:S(2)}) collective-permute-start(bf16[384,512]{1,0:T(8,128)(2,1)S(1)} %collective-permute-done.23.refs_0_), channel_id=1, source_target_pairs={{0,4},{4,0},{8,12},{12,8},{16,20},{20,16},{24,28},{28,24},{1,5},{5... | collective-permute-start | bytes 1179656 | tf_op jit(solution)/shard_map/ppermute | solution.py:31
  113.0 12.1 %collective-permute-start.15 = (bf16[384,512]{1,0:T(8,128)(2,1)S(1)}, bf16[384,512]{1,0:T(8,128)(2,1)S(1)}, u32[]{:S(2)}, u32[]{:S(2)}) collective-permute-start(bf16[384,512]{1,0:T(8,128)(2,1)S(1)} %bitcast.32), channel_id=1, source_target_pairs={{0,1},{1,0},{2,3},{3,2},{4,5},{5,4},{6,7},{7,6},{8,9},{9,8},{10,11... | collective-permute-start | bytes 1179656 | tf_op jit(solution)/shard_map/ppermute | solution.py:43
  114.6 12.2 %collective-permute-start.34 = (bf16[384,512]{1,0:T(8,128)(2,1)S(1)}, bf16[384,512]{1,0:T(8,128)(2,1)S(1)}, u32[]{:S(2)}, u32[]{:S(2)}) collective-permute-start(bf16[384,512]{1,0:T(8,128)(2,1)S(1)} %collective-permute-done.33.refs_0_), channel_id=1, source_target_pairs={{0,4},{4,0},{8,12},{12,8},{16,20},{20,16},{24,28},{28,24},{1,5},{5... | collective-permute-start | bytes 1179656 | tf_op jit(solution)/shard_map/ppermute | solution.py:31
  115.2 12.3 %collective-permute-start.45 = (bf16[384,512]{1,0:T(8,128)(2,1)S(1)}, bf16[384,512]{1,0:T(8,128)(2,1)S(1)}, u32[]{:S(2)}, u32[]{:S(2)}) collective-permute-start(bf16[384,512]{1,0:T(8,128)(2,1)S(1)} %bitcast.38), channel_id=1, source_target_pairs={{0,2},{1,3},{2,0},{3,1},{4,6},{5,7},{6,4},{7,5},{8,10},{9,11},{10,... | collective-permute-start | bytes 1179656 | tf_op jit(solution)/shard_map/ppermute | solution.py:43
  115.8 17.7 %collective-permute-start.44 = (bf16[384,512]{1,0:T(8,128)(2,1)S(1)}, bf16[384,512]{1,0:T(8,128)(2,1)S(1)}, u32[]{:S(2)}, u32[]{:S(2)}) collective-permute-start(bf16[384,512]{1,0:T(8,128)(2,1)S(1)} %bitcast.39), channel_id=1, source_target_pairs={{0,1},{1,0},{2,3},{3,2},{4,5},{5,4},{6,7},{7,6},{8,9},{9,8},{10,11... | collective-permute-start | bytes 1179656 | tf_op jit(solution)/shard_map/ppermute | solution.py:43
  117.5 18.2 %collective-permute-start.16 = (bf16[384,512]{1,0:T(8,128)(2,1)S(1)}, bf16[384,512]{1,0:T(8,128)(2,1)S(1)}, u32[]{:S(2)}, u32[]{:S(2)}) collective-permute-start(bf16[384,512]{1,0:T(8,128)(2,1)S(1)} %bitcast.33), channel_id=1, source_target_pairs={{0,2},{1,3},{2,0},{3,1},{4,6},{5,7},{6,4},{7,5},{8,10},{9,11},{10,... | collective-permute-start | bytes 1179656 | tf_op jit(solution)/shard_map/ppermute | solution.py:43
  125.1 19.0 %collective-permute-start.26 = (bf16[384,512]{1,0:T(8,128)(2,1)S(1)}, bf16[384,512]{1,0:T(8,128)(2,1)S(1)}, u32[]{:S(2)}, u32[]{:S(2)}) collective-permute-start(bf16[384,512]{1,0:T(8,128)(2,1)S(1)} %bitcast.35), channel_id=1, source_target_pairs={{0,2},{1,3},{2,0},{3,1},{4,6},{5,7},{6,4},{7,5},{8,10},{9,11},{10,... | collective-permute-start | bytes 1179656 | tf_op jit(solution)/shard_map/ppermute | solution.py:43
  126.8 25.7 %collective-permute-start.17 = (bf16[384,512]{1,0:T(8,128)(2,1)S(1)}, bf16[384,512]{1,0:T(8,128)(2,1)S(1)}, u32[]{:S(2)}, u32[]{:S(2)}) collective-permute-start(bf16[384,512]{1,0:T(8,128)(2,1)S(1)} %collective-permute-done.15.refs_1_), channel_id=1, source_target_pairs={{0,2},{1,3},{2,0},{3,1},{4,6},{5,7},{6,4},{7,5},{8,10},{9,11},{10,... | collective-permute-start | bytes 1179656 | tf_op jit(solution)/shard_map/ppermute | solution.py:43
  127.5 25.5 %collective-permute-start.35 = (bf16[384,512]{1,0:T(8,128)(2,1)S(1)}, bf16[384,512]{1,0:T(8,128)(2,1)S(1)}, u32[]{:S(2)}, u32[]{:S(2)}) collective-permute-start(bf16[384,512]{1,0:T(8,128)(2,1)S(1)} %bitcast.29), channel_id=1, source_target_pairs={{0,1},{1,0},{2,3},{3,2},{4,5},{5,4},{6,7},{7,6},{8,9},{9,8},{10,11... | collective-permute-start | bytes 1179656 | tf_op jit(solution)/shard_map/ppermute | solution.py:43
  133.5 26.6 %collective-permute-start.46 = (bf16[384,512]{1,0:T(8,128)(2,1)S(1)}, bf16[384,512]{1,0:T(8,128)(2,1)S(1)}, u32[]{:S(2)}, u32[]{:S(2)}) collective-permute-start(bf16[384,512]{1,0:T(8,128)(2,1)S(1)} %collective-permute-done.45.refs_2_), channel_id=1, source_target_pairs={{0,1},{1,0},{2,3},{3,2},{4,5},{5,4},{6,7},{7,6},{8,9},{9,8},{10,11... | collective-permute-start | bytes 1179656 | tf_op jit(solution)/shard_map/ppermute | solution.py:43
  135.7 27.6 %collective-permute-start.25 = (bf16[384,512]{1,0:T(8,128)(2,1)S(1)}, bf16[384,512]{1,0:T(8,128)(2,1)S(1)}, u32[]{:S(2)}, u32[]{:S(2)}) collective-permute-start(bf16[384,512]{1,0:T(8,128)(2,1)S(1)} %bitcast.36), channel_id=1, source_target_pairs={{0,1},{1,0},{2,3},{3,2},{4,5},{5,4},{6,7},{7,6},{8,9},{9,8},{10,11... | collective-permute-start | bytes 1179656 | tf_op jit(solution)/shard_map/ppermute | solution.py:43
  144.1 30.1 %collective-permute-start.36 = (bf16[384,512]{1,0:T(8,128)(2,1)S(1)}, bf16[384,512]{1,0:T(8,128)(2,1)S(1)}, u32[]{:S(2)}, u32[]{:S(2)}) collective-permute-start(bf16[384,512]{1,0:T(8,128)(2,1)S(1)} %bitcast.30), channel_id=1, source_target_pairs={{0,2},{1,3},{2,0},{3,1},{4,6},{5,7},{6,4},{7,5},{8,10},{9,11},{10,... | collective-permute-start | bytes 1179656 | tf_op jit(solution)/shard_map/ppermute | solution.py:43
  152.5 14.7 %collective-permute-start.27 = (bf16[384,512]{1,0:T(8,128)(2,1)S(1)}, bf16[384,512]{1,0:T(8,128)(2,1)S(1)}, u32[]{:S(2)}, u32[]{:S(2)}) collective-permute-start(bf16[384,512]{1,0:T(8,128)(2,1)S(1)} %collective-permute-done.26.refs_2_), channel_id=1, source_target_pairs={{0,1},{1,0},{2,3},{3,2},{4,5},{5,4},{6,7},{7,6},{8,9},{9,8},{10,11... | collective-permute-start | bytes 1179656 | tf_op jit(solution)/shard_map/ppermute | solution.py:43
  153.0 22.8 %collective-permute-start.37 = (bf16[384,512]{1,0:T(8,128)(2,1)S(1)}, bf16[384,512]{1,0:T(8,128)(2,1)S(1)}, u32[]{:S(2)}, u32[]{:S(2)}) collective-permute-start(bf16[384,512]{1,0:T(8,128)(2,1)S(1)} %collective-permute-done.35.refs_1_), channel_id=1, source_target_pairs={{0,2},{1,3},{2,0},{3,1},{4,6},{5,7},{6,4},{7,5},{8,10},{9,11},{10,... | collective-permute-start | bytes 1179656 | tf_op jit(solution)/shard_map/ppermute | solution.py:43
  160.1 13.5 %collective-permute-start.19 = (bf16[384,256]{1,0:T(8,128)(2,1)S(1)}, bf16[384,256]{1,0:T(8,128)(2,1)S(1)}, u32[]{:S(2)}, u32[]{:S(2)}) collective-permute-start(bf16[384,256]{1,0:T(8,128)(2,1)S(1)} %hidden_units.4.refs_0_), channel_id=1, source_target_pairs={{0,2},{1,3},{2,0},{3,1},{4,6},{5,7},{6,4},{7,5},{8,10},{9,11},{10,... | collective-permute-start | bytes 589832 | tf_op jit(solution)/shard_map/ppermute | solution.py:43
  163.2 15.7 %collective-permute-start.47 = (bf16[384,256]{1,0:T(8,128)(2,1)S(1)}, bf16[384,256]{1,0:T(8,128)(2,1)S(1)}, u32[]{:S(2)}, u32[]{:S(2)}) collective-permute-start(bf16[384,256]{1,0:T(8,128)(2,1)S(1)} %hidden_units.7.refs_0_), channel_id=1, source_target_pairs={{0,1},{1,0},{2,3},{3,2},{4,5},{5,4},{6,7},{7,6},{8,9},{9,8},{10,11... | collective-permute-start | bytes 589832 | tf_op jit(solution)/shard_map/ppermute | solution.py:43
  167.2 13.3 %collective-permute-start.48 = (bf16[384,256]{1,0:T(8,128)(2,1)S(1)}, bf16[384,256]{1,0:T(8,128)(2,1)S(1)}, u32[]{:S(2)}, u32[]{:S(2)}) collective-permute-start(bf16[384,256]{1,0:T(8,128)(2,1)S(1)} %hidden_units.7.refs_0_), channel_id=1, source_target_pairs={{0,2},{1,3},{2,0},{3,1},{4,6},{5,7},{6,4},{7,5},{8,10},{9,11},{10,... | collective-permute-start | bytes 589832 | tf_op jit(solution)/shard_map/ppermute | solution.py:43
  173.6 8.4 %collective-permute-start.29 = (bf16[384,256]{1,0:T(8,128)(2,1)S(1)}, bf16[384,256]{1,0:T(8,128)(2,1)S(1)}, u32[]{:S(2)}, u32[]{:S(2)}) collective-permute-start(bf16[384,256]{1,0:T(8,128)(2,1)S(1)} %hidden_units.5.refs_0_), channel_id=1, source_target_pairs={{0,2},{1,3},{2,0},{3,1},{4,6},{5,7},{6,4},{7,5},{8,10},{9,11},{10,... | collective-permute-start | bytes 589832 | tf_op jit(solution)/shard_map/ppermute | solution.py:43
  174.2 8.4 %collective-permute-start.18 = (bf16[384,256]{1,0:T(8,128)(2,1)S(1)}, bf16[384,256]{1,0:T(8,128)(2,1)S(1)}, u32[]{:S(2)}, u32[]{:S(2)}) collective-permute-start(bf16[384,256]{1,0:T(8,128)(2,1)S(1)} %hidden_units.4.refs_0_), channel_id=1, source_target_pairs={{0,1},{1,0},{2,3},{3,2},{4,5},{5,4},{6,7},{7,6},{8,9},{9,8},{10,11... | collective-permute-start | bytes 589832 | tf_op jit(solution)/shard_map/ppermute | solution.py:43
  175.8 10.3 %collective-permute-start.20 = (bf16[384,256]{1,0:T(8,128)(2,1)S(1)}, bf16[384,256]{1,0:T(8,128)(2,1)S(1)}, u32[]{:S(2)}, u32[]{:S(2)}) collective-permute-start(bf16[384,256]{1,0:T(8,128)(2,1)S(1)} %collective-permute-done.19.refs_2_), channel_id=1, source_target_pairs={{0,1},{1,0},{2,3},{3,2},{4,5},{5,4},{6,7},{7,6},{8,9},{9,8},{10,11... | collective-permute-start | bytes 589832 | tf_op jit(solution)/shard_map/ppermute | solution.py:43
  179.0 8.8 %collective-permute-start.39 = (bf16[384,256]{1,0:T(8,128)(2,1)S(1)}, bf16[384,256]{1,0:T(8,128)(2,1)S(1)}, u32[]{:S(2)}, u32[]{:S(2)}) collective-permute-start(bf16[384,256]{1,0:T(8,128)(2,1)S(1)} %hidden_units.6.refs_0_), channel_id=1, source_target_pairs={{0,2},{1,3},{2,0},{3,1},{4,6},{5,7},{6,4},{7,5},{8,10},{9,11},{10,... | collective-permute-start | bytes 589832 | tf_op jit(solution)/shard_map/ppermute | solution.py:43
  180.5 9.9 %collective-permute-start.28 = (bf16[384,256]{1,0:T(8,128)(2,1)S(1)}, bf16[384,256]{1,0:T(8,128)(2,1)S(1)}, u32[]{:S(2)}, u32[]{:S(2)}) collective-permute-start(bf16[384,256]{1,0:T(8,128)(2,1)S(1)} %hidden_units.5.refs_0_), channel_id=1, source_target_pairs={{0,1},{1,0},{2,3},{3,2},{4,5},{5,4},{6,7},{7,6},{8,9},{9,8},{10,11... | collective-permute-start | bytes 589832 | tf_op jit(solution)/shard_map/ppermute | solution.py:43
  182.0 12.6 %collective-permute-start.30 = (bf16[384,256]{1,0:T(8,128)(2,1)S(1)}, bf16[384,256]{1,0:T(8,128)(2,1)S(1)}, u32[]{:S(2)}, u32[]{:S(2)}) collective-permute-start(bf16[384,256]{1,0:T(8,128)(2,1)S(1)} %collective-permute-done.29.refs_2_), channel_id=1, source_target_pairs={{0,1},{1,0},{2,3},{3,2},{4,5},{5,4},{6,7},{7,6},{8,9},{9,8},{10,11... | collective-permute-start | bytes 589832 | tf_op jit(solution)/shard_map/ppermute | solution.py:43
  182.5 13.3 %collective-permute-start.49 = (bf16[384,256]{1,0:T(8,128)(2,1)S(1)}, bf16[384,256]{1,0:T(8,128)(2,1)S(1)}, u32[]{:S(2)}, u32[]{:S(2)}) collective-permute-start(bf16[384,256]{1,0:T(8,128)(2,1)S(1)} %collective-permute-done.47.refs_1_), channel_id=1, source_target_pairs={{0,2},{1,3},{2,0},{3,1},{4,6},{5,7},{6,4},{7,5},{8,10},{9,11},{10,... | collective-permute-start | bytes 589832 | tf_op jit(solution)/shard_map/ppermute | solution.py:43
  186.2 12.2 %collective-permute-start.38 = (bf16[384,256]{1,0:T(8,128)(2,1)S(1)}, bf16[384,256]{1,0:T(8,128)(2,1)S(1)}, u32[]{:S(2)}, u32[]{:S(2)}) collective-permute-start(bf16[384,256]{1,0:T(8,128)(2,1)S(1)} %hidden_units.6.refs_0_), channel_id=1, source_target_pairs={{0,1},{1,0},{2,3},{3,2},{4,5},{5,4},{6,7},{7,6},{8,9},{9,8},{10,11... | collective-permute-start | bytes 589832 | tf_op jit(solution)/shard_map/ppermute | solution.py:43
  187.8 13.5 %collective-permute-start.40 = (bf16[384,256]{1,0:T(8,128)(2,1)S(1)}, bf16[384,256]{1,0:T(8,128)(2,1)S(1)}, u32[]{:S(2)}, u32[]{:S(2)}) collective-permute-start(bf16[384,256]{1,0:T(8,128)(2,1)S(1)} %collective-permute-done.39.refs_2_), channel_id=1, source_target_pairs={{0,1},{1,0},{2,3},{3,2},{4,5},{5,4},{6,7},{7,6},{8,9},{9,8},{10,11... | collective-permute-start | bytes 589832 | tf_op jit(solution)/shard_map/ppermute | solution.py:43
  190.4 12.3 %collective-permute-start.21 = (bf16[192,512]{1,0:T(8,128)(2,1)S(1)}, bf16[192,512]{1,0:T(8,128)(2,1)S(1)}, u32[]{:S(2)}, u32[]{:S(2)}) collective-permute-start(bf16[192,512]{1,0:T(8,128)(2,1)S(1)} %get-tuple-element.33), channel_id=1, source_target_pairs={{0,24},{4,28},{8,0},{12,4},{16,8},{20,12},{24,16},{28,20},{1,25},{... | collective-permute-start | bytes 589832 | tf_op jit(solution)/shard_map/ppermute | solution.py:36
  194.6 8.9 %collective-permute-start.22 = (bf16[192,512]{1,0:T(8,128)(2,1)S(1)}, bf16[192,512]{1,0:T(8,128)(2,1)S(1)}, u32[]{:S(2)}, u32[]{:S(2)}) collective-permute-start(bf16[192,512]{1,0:T(8,128)(2,1)S(1)} %get-tuple-element.34), channel_id=1, source_target_pairs={{0,28},{4,24},{8,4},{12,0},{16,12},{20,8},{24,20},{28,16},{1,29},{... | collective-permute-start | bytes 589832 | tf_op jit(solution)/shard_map/ppermute | solution.py:36
  195.8 25.2 %collective-permute-start.31 = (bf16[192,512]{1,0:T(8,128)(2,1)S(1)}, bf16[192,512]{1,0:T(8,128)(2,1)S(1)}, u32[]{:S(2)}, u32[]{:S(2)}) collective-permute-start(bf16[192,512]{1,0:T(8,128)(2,1)S(1)} %get-tuple-element.35), channel_id=1, source_target_pairs={{0,16},{4,20},{8,24},{12,28},{16,0},{20,4},{24,8},{28,12},{1,17},{... | collective-permute-start | bytes 589832 | tf_op jit(solution)/shard_map/ppermute | solution.py:36
  198.3 27.0 %collective-permute-start.32 = (bf16[192,512]{1,0:T(8,128)(2,1)S(1)}, bf16[192,512]{1,0:T(8,128)(2,1)S(1)}, u32[]{:S(2)}, u32[]{:S(2)}) collective-permute-start(bf16[192,512]{1,0:T(8,128)(2,1)S(1)} %get-tuple-element.36), channel_id=1, source_target_pairs={{0,20},{4,16},{8,28},{12,24},{16,4},{20,0},{24,12},{28,8},{1,21},{... | collective-permute-start | bytes 589832 | tf_op jit(solution)/shard_map/ppermute | solution.py:36
  201.3 25.0 %collective-permute-start.50 = (bf16[192,512]{1,0:T(8,128)(2,1)S(1)}, bf16[192,512]{1,0:T(8,128)(2,1)S(1)}, u32[]{:S(2)}, u32[]{:S(2)}) collective-permute-start(bf16[192,512]{1,0:T(8,128)(2,1)S(1)} %get-tuple-element.42), channel_id=1, source_target_pairs={{0,4},{4,0},{8,12},{12,8},{16,20},{20,16},{24,28},{28,24},{1,5},{5... | collective-permute-start | bytes 589832 | tf_op jit(solution)/shard_map/ppermute | solution.py:36
  202.7 23.7 %collective-permute-start.41 = (bf16[192,512]{1,0:T(8,128)(2,1)S(1)}, bf16[192,512]{1,0:T(8,128)(2,1)S(1)}, u32[]{:S(2)}, u32[]{:S(2)}) collective-permute-start(bf16[192,512]{1,0:T(8,128)(2,1)S(1)} %get-tuple-element.39), channel_id=1, source_target_pairs={{0,8},{4,12},{8,16},{12,20},{16,24},{20,28},{24,0},{28,4},{1,9},{5... | collective-permute-start | bytes 589832 | tf_op jit(solution)/shard_map/ppermute | solution.py:36
  203.5 22.9 %collective-permute-start.42 = (bf16[192,512]{1,0:T(8,128)(2,1)S(1)}, bf16[192,512]{1,0:T(8,128)(2,1)S(1)}, u32[]{:S(2)}, u32[]{:S(2)}) collective-permute-start(bf16[192,512]{1,0:T(8,128)(2,1)S(1)} %get-tuple-element.40), channel_id=1, source_target_pairs={{0,12},{4,8},{8,20},{12,16},{16,28},{20,24},{24,4},{28,0},{1,13},{... | collective-permute-start | bytes 589832 | tf_op jit(solution)/shard_map/ppermute | solution.py:36
  (19 other events, 225.5 us)

commit v2 on v1

--- a/solution.py
+++ b/solution.py
@@ -634,16 +634,15 @@
                 if k or side:
                     home = move_chips(home, -k, bool(side))
                 returned.append((2 * k + side, home))
-    returned = returned[2:-2] + returned[-2:] + returned[:2]
-    late = 4
     total = kept
-    for part, kind in ((returned[:-late], jnp.float32), (returned[-late:], jnp.bfloat16)):
+    parts = (returned[2:-2], returned[:2], returned[-2:])
+    for part, kind in zip(parts, (jnp.float32, jnp.float32, jnp.bfloat16)):
         places, rows = zip(*part)
         total = combine(total, rows, places, leave_ranks, shares, kind)
     return total
 
 
-RELAYS = ((2, 1), (1, 2), (2, 2), (1, 2))
+RELAYS = ((1, 1), (2, 1), (1, 1), (2, 2))
 
 
 def solution(mesh):

time: 229 us -> 233 us (1.017)
  waiting for transfers between devices: 117 us -> 120 us
  transfers between devices with their start and end apart: 51 -> 51, of which waited for: 26 -> 27; matrix products, arithmetic and copies ran while one was open for 1% -> 1% of each run, Pallas kernels for 11% -> 11%
where the time goes in v2:
time: 233 us
  waiting for transfers between devices  120 us (52%)
  starting transfers between devices  59.4 us (25%)
  Pallas kernels  37.5 us (16%)
  local copies, waits for them, and re-layouts  12.6 us (5%)
  other arithmetic  2.63 us (1%)
    ppermute x27, waiting for transfers between devices, swap_tp(): return lax.ppermute(value, 'tp', [(i, i ^ mask) for i in range(count)])  56.9 us
    ppermute x13, waiting for transfers between devices, move_chips(): lax.ppermute(value, 'sp', [(i, (i + 2 * steps) % count ^ int(cross)) for...  55.4 us
    ppermute x27, starting transfers between devices, swap_tp(): return lax.ppermute(value, 'tp', [(i, i ^ mask) for i in range(count)])  29.5 us
    ppermute x13, starting transfers between devices, move_chips(): lax.ppermute(value, 'sp', [(i, (i + 2 * steps) % count ^ int(cross)) for...  15.2 us
    pallas_call x4, Pallas kernels, hidden_units(): pl.pallas_call(kernel, grid_spec=pltpu.PrefetchScalarGridSpec(num_scalar_...  10.9 us
    unnamed x33, local copies, waits for them, and re-layouts  8.9 us
    ppermute x3, starting transfers between devices, sent_states(): sent.append(lax.ppermute(chip, 'sp', pairs))  8.62 us
    pallas_call x1, Pallas kernels, mixer_local(): pl.pallas_call(kernel, grid=(groups,), in_specs=[pl.BlockSpec((length, st...  5.91 us
  transfers between devices with their start and end apart: 51, of which 27 were waited for; matrix products, arithmetic and copies ran while one was open for 1% of the time, Pallas kernels for 11%

profile of v2, /device:TPU:0, one launch (start us, length us, event | category | flops | bytes accessed | tf_op | source)
XLA Modules:
  0.0 232.5 jit_solution(12886148276142797390)
XLA Ops:
  2.2 2.4 %collective-permute-start = (bf16[16,2048]{1,0:T(8,128)(2,1)S(1)}, bf16[16,2048]{1,0:T(8,128)(2,1)S(1)}, u32[]{:S(2)}, u32[]{:S(2)}) collective-permute-start(bf16[16,2048]{1,0:T(8,128)(2,1)S(1)} %pad_maximum_fusion.1), channel_id=1, source_target_pairs={{0,4},{4,8},{8,12},{12,16},{16,20},{20,24},{24,28},{1,5},{5,9},{9,... | collective-permute-start | bytes 196616 | tf_op jit(solution)/shard_map/ppermute | solution.py:22
  7.7 5.8 %mixer_states.1 = (bf16[384,1024]{1,0:T(8,128)(2,1)}, bf16[384,512]{1,0:T(8,128)(2,1)}, f32[16,384]{1,0:T(8,128)}, f32[16,384]{1,0:T(8,128)}, bf16[384,1024]{1,0:T(8,128)(2,1)}, /*index=5*/bf16[144,1024]{1,0:T(8,128)(2,1)}) custom-call(bf16[384,1024]{1,0:T(8,128)(2,1)} %act_ref.1, bf16[384,1024]{1,0:T(8,128)(2,1)} %copy-done.12, ...), custom_call_target="tpu_custom_call" | custom-call | tf_op jit(solution)/shard_map/mixer_states/pallas_call | solution.py:347
  13.4 2.7 %collective-permute-start.1 = (bf16[144,1024]{1,0:T(8,128)(2,1)}, bf16[144,1024]{1,0:T(8,128)(2,1)S(1)}, u32[]{:S(2)}, u32[]{:S(2)}) collective-permute-start(bf16[144,1024]{1,0:T(8,128)(2,1)} %get-tuple-element.31), channel_id=1, source_target_pairs={{0,4},{4,0},{8,12},{12,8},{16,20},{20,16},{24,28},{28,24},{1,5},{5... | collective-permute-start | bytes 884744 | tf_op jit(solution)/shard_map/ppermute | solution.py:31
  18.7 3.5 %collective-permute-start.2 = (bf16[144,512]{1,0:T(8,128)(2,1)S(1)}, bf16[144,512]{1,0:T(8,128)(2,1)S(1)}, u32[]{:S(2)}, u32[]{:S(2)}) collective-permute-start(bf16[144,512]{1,0:T(8,128)(2,1)S(1)} %pad_maximum_fusion), channel_id=1, source_target_pairs={{0,8},{4,12},{8,16},{12,20},{16,24},{20,28},{1,9},{5,13},{9,17},{1... | collective-permute-start | bytes 442376 | tf_op jit(solution)/shard_map/ppermute | solution.py:502
  22.2 3.3 %collective-permute-start.4 = (bf16[144,512]{1,0:T(8,128)(2,1)S(1)}, bf16[144,512]{1,0:T(8,128)(2,1)S(1)}, u32[]{:S(2)}, u32[]{:S(2)}) collective-permute-start(bf16[144,512]{1,0:T(8,128)(2,1)S(1)} %pad_maximum_fusion), channel_id=1, source_target_pairs={{0,24},{4,28},{1,25},{5,29},{2,26},{6,30},{3,27},{7,31}} | collective-permute-start | bytes 442376 | tf_op jit(solution)/shard_map/ppermute | solution.py:502
  25.5 1.9 collective-permute-start.3
  27.4 2.3 %collective-permute-done.4 = bf16[144,512]{1,0:T(8,128)(2,1)S(1)} collective-permute-done((bf16[144,512]{1,0:T(8,128)(2,1)S(1)}, bf16[144,512]{1,0:T(8,128)(2,1)S(1)}, u32[]{:S(2)}, u32[]{:S(2)}) %collective-permute-start.4) | collective-permute-done | bytes 147488 | tf_op jit(solution)/shard_map/ppermute | solution.py:502
  29.8 2.4 %collective-permute-done.3 = bf16[144,512]{1,0:T(8,128)(2,1)S(1)} collective-permute-done((bf16[144,512]{1,0:T(8,128)(2,1)S(1)}, bf16[144,512]{1,0:T(8,128)(2,1)S(1)}, u32[]{:S(2)}, u32[]{:S(2)}) %collective-permute-start.3) | collective-permute-done | bytes 147488 | tf_op jit(solution)/shard_map/ppermute | solution.py:502
  32.4 5.9 %mixer_local.1 = (f32[384,1024]{1,0:T(8,128)}, bf16[384,512]{1,0:T(8,128)(2,1)}) custom-call(bf16[384,1024]{1,0:T(8,128)(2,1)} %copy-done.12, bf16[16,2048]{1,0:T(8,128)(2,1)} %copy-done.13, bf16[4,4,128]{2,1,0:T(4,128)(2,1)} %taps_ref.3, bf16[384,1024]{1,0:T(8,128)(2,1)} %get-tuple-element.24.value_ref, bf16[384,512]{1,0:T(8,128)(2,1)} %get-tuple-element.25.write_ref, ...), custom_call_target="tpu_custom_call" | custom-call | flops 4000000000 | bytes 4000000 | tf_op jit(solution)/shard_map/mixer_local/pallas_call | solution.py:408
  38.6 1.5 copy-done.6
  41.1 2.9 %mixer_mix.1.mixed_ref = bf16[384,1024]{1,0:T(8,128)(2,1)S(1)} custom-call(f32[384,1024]{1,0:T(8,128)S(1)} %copy-done.6, bf16[384,512]{1,0:T(8,128)(2,1)S(1)} %copy-done.8, f32[16,384]{1,0:T(8,128)S(1)} %copy-done.9, bf16[128,1024]{1,0:T(8,128)(2,1)S(1)} %fusion.1.arrive_ref, bf16[384,1024]{1,0:T(8,128)(2,1)S(1)} %copy-done.7, f32[1,1024]{1,0:T(1,128)S(1)} %bitcast.41), custom_call_target="tpu_custom_call" | custom-call | tf_op jit(solution)/shard_map/mixer_mix/pallas_call | solution.py:448
  45.8 2.5 %collective-permute-start.6 = (bf16[384,512]{1,0:T(8,128)(2,1)S(1)}, bf16[384,512]{1,0:T(8,128)(2,1)S(1)}, u32[]{:S(2)}, u32[]{:S(2)}) collective-permute-start(bf16[384,512]{1,0:T(8,128)(2,1)S(1)} %project_share.5), channel_id=1, source_target_pairs={{0,3},{1,2},{2,1},{3,0},{4,7},{5,6},{6,5},{7,4},{8,11},{9,10},{10,... | collective-permute-start | bytes 1179656 | tf_op jit(solution)/shard_map/ppermute | solution.py:43
  49.5 2.2 copy-done.2
  52.2 6.6 %collective-permute-done.6 = bf16[384,512]{1,0:T(8,128)(2,1)S(1)} collective-permute-done((bf16[384,512]{1,0:T(8,128)(2,1)S(1)}, bf16[384,512]{1,0:T(8,128)(2,1)S(1)}, u32[]{:S(2)}, u32[]{:S(2)}) %collective-permute-start.6) | collective-permute-done | bytes 393248 | tf_op jit(solution)/shard_map/ppermute | solution.py:43
  58.8 7.9 %collective-permute-done.7 = bf16[384,512]{1,0:T(8,128)(2,1)S(1)} collective-permute-done((bf16[384,512]{1,0:T(8,128)(2,1)S(1)}, bf16[384,512]{1,0:T(8,128)(2,1)S(1)}, u32[]{:S(2)}, u32[]{:S(2)}) %collective-permute-start.7) | collective-permute-done | bytes 393248 | tf_op jit(solution)/shard_map/ppermute | solution.py:43
  68.1 4.7 %collective-permute-start.9 = (bf16[384,512]{1,0:T(8,128)(2,1)S(1)}, bf16[384,512]{1,0:T(8,128)(2,1)S(1)}, u32[]{:S(2)}, u32[]{:S(2)}) collective-permute-start(bf16[384,512]{1,0:T(8,128)(2,1)S(1)} %get-tuple-element.43.refs_0_), channel_id=1, source_target_pairs={{0,8},{4,12},{8,16},{12,20},{16,24},{20,28},{24,0},{28,4},{1,9},{5... | collective-permute-start | bytes 1179656 | tf_op jit(solution)/shard_map/ppermute | solution.py:36
  72.8 12.0 %collective-permute-done.9.refs_0_ = bf16[384,512]{1,0:T(8,128)(2,1)S(1)} collective-permute-done((bf16[384,512]{1,0:T(8,128)(2,1)S(1)}, bf16[384,512]{1,0:T(8,128)(2,1)S(1)}, u32[]{:S(2)}, u32[]{:S(2)}) %collective-permute-start.9) | collective-permute-done | bytes 393248 | tf_op jit(solution)/shard_map/ppermute | solution.py:36
  84.9 12.2 %collective-permute-done.23.refs_0_ = bf16[384,512]{1,0:T(8,128)(2,1)S(1)} collective-permute-done((bf16[384,512]{1,0:T(8,128)(2,1)S(1)}, bf16[384,512]{1,0:T(8,128)(2,1)S(1)}, u32[]{:S(2)}, u32[]{:S(2)}) %collective-permute-start.23) | collective-permute-done | bytes 393248 | tf_op jit(solution)/shard_map/ppermute | solution.py:36
  98.8 4.4 %collective-permute-start.13 = (s32[4,384]{1,0:T(4,128)S(1)}, s32[4,384]{1,0:T(4,128)S(1)}, u32[]{:S(2)}, u32[]{:S(2)}) collective-permute-start(s32[4,384]{1,0:T(4,128)S(1)} %pad_add_fusion), channel_id=1, source_target_pairs={{0,16},{4,20},{8,24},{12,28},{16,0},{20,4},{24,8},{28,12},{1,17},{... | collective-permute-start | bytes 18440 | tf_op jit(solution)/shard_map/ppermute | solution.py:36
  103.2 5.5 %collective-permute-done.12 = s32[4,384]{1,0:T(4,128)S(1)} collective-permute-done((s32[4,384]{1,0:T(4,128)S(1)}, s32[4,384]{1,0:T(4,128)S(1)}, u32[]{:S(2)}, u32[]{:S(2)}) %collective-permute-start.12) | collective-permute-done | bytes 6176 | tf_op jit(solution)/shard_map/ppermute | solution.py:36
  108.8 3.5 %collective-permute-done.14 = s32[4,384]{1,0:T(4,128)S(1)} collective-permute-done((s32[4,384]{1,0:T(4,128)S(1)}, s32[4,384]{1,0:T(4,128)S(1)}, u32[]{:S(2)}, u32[]{:S(2)}) %collective-permute-start.14) | collective-permute-done | bytes 6176 | tf_op jit(solution)/shard_map/ppermute | solution.py:36
  113.0 1.8 collective-permute-start.16
  115.6 1.7 collective-permute-start.35
  118.2 6.9 %collective-permute-done.16.refs_2_ = bf16[384,512]{1,0:T(8,128)(2,1)S(1)} collective-permute-done((bf16[384,512]{1,0:T(8,128)(2,1)S(1)}, bf16[384,512]{1,0:T(8,128)(2,1)S(1)}, u32[]{:S(2)}, u32[]{:S(2)}) %collective-permute-start.16) | collective-permute-done | bytes 393248 | tf_op jit(solution)/shard_map/ppermute | solution.py:43
  127.5 1.8 collective-permute-start.44
  129.3 4.2 %collective-permute-done.35.refs_2_ = bf16[384,512]{1,0:T(8,128)(2,1)S(1)} collective-permute-done((bf16[384,512]{1,0:T(8,128)(2,1)S(1)}, bf16[384,512]{1,0:T(8,128)(2,1)S(1)}, u32[]{:S(2)}, u32[]{:S(2)}) %collective-permute-start.35) | collective-permute-done | bytes 393248 | tf_op jit(solution)/shard_map/ppermute | solution.py:43
  133.5 1.7 collective-permute-start.36
  136.2 8.1 %collective-permute-done.25.refs_1_ = bf16[384,512]{1,0:T(8,128)(2,1)S(1)} collective-permute-done((bf16[384,512]{1,0:T(8,128)(2,1)S(1)}, bf16[384,512]{1,0:T(8,128)(2,1)S(1)}, u32[]{:S(2)}, u32[]{:S(2)}) %collective-permute-start.25) | collective-permute-done | bytes 393248 | tf_op jit(solution)/shard_map/ppermute | solution.py:43
  144.4 8.3 %collective-permute-done.17.refs_3_ = bf16[384,512]{1,0:T(8,128)(2,1)S(1)} collective-permute-done((bf16[384,512]{1,0:T(8,128)(2,1)S(1)}, bf16[384,512]{1,0:T(8,128)(2,1)S(1)}, u32[]{:S(2)}, u32[]{:S(2)}) %collective-permute-start.17) | collective-permute-done | bytes 393248 | tf_op jit(solution)/shard_map/ppermute | solution.py:43
  154.9 2.2 copy-done.4
  157.1 2.7 %hidden_units.4.refs_0_ = bf16[384,256]{1,0:T(8,128)(2,1)S(1)} custom-call(s32[1]{0:T(128)} %bitcast.own_ref, bf16[384,512]{1,0:T(8,128)(2,1)S(1)} %bitcast.34, bf16[384,512]{1,0:T(8,128)(2,1)S(1)} %collective-permute-done.15.refs_1_, bf16[384,512]{1,0:T(8,128)(2,1)S(1)} %collective-permute-done.16.refs_2_, ...), custom_call_target="tpu_custom_call" | custom-call | flops 805306368 | bytes 8388608 | tf_op jit(solution)/shard_map/hidden_units/pallas_call | solution.py:151
  160.5 2.7 %hidden_units.6.refs_0_ = bf16[384,256]{1,0:T(8,128)(2,1)S(1)} custom-call(s32[1]{0:T(128)} %bitcast.own_ref, bf16[384,512]{1,0:T(8,128)(2,1)S(1)} %bitcast.40, bf16[384,512]{1,0:T(8,128)(2,1)S(1)} %collective-permute-done.34.refs_1_, bf16[384,512]{1,0:T(8,128)(2,1)S(1)} %collective-permute-done.35.refs_2_, ...), custom_call_target="tpu_custom_call" | custom-call | flops 805306368 | bytes 8388608 | tf_op jit(solution)/shard_map/hidden_units/pallas_call | solution.py:151
  164.8 2.0 collective-permute-done.27.refs_3_
  166.7 1.7 collective-permute-start.38
  168.4 2.7 %hidden_units.5.refs_0_ = bf16[384,256]{1,0:T(8,128)(2,1)S(1)} custom-call(s32[1]{0:T(128)} %bitcast.own_ref, bf16[384,512]{1,0:T(8,128)(2,1)S(1)} %bitcast.37, bf16[384,512]{1,0:T(8,128)(2,1)S(1)} %collective-permute-done.25.refs_1_, bf16[384,512]{1,0:T(8,128)(2,1)S(1)} %collective-permute-done.26.refs_2_, ...), custom_call_target="tpu_custom_call" | custom-call | flops 805306368 | bytes 8388608 | tf_op jit(solution)/shard_map/hidden_units/pallas_call | solution.py:151
  171.2 2.6 %collective-permute-done.18.refs_1_ = bf16[384,256]{1,0:T(8,128)(2,1)S(1)} collective-permute-done((bf16[384,256]{1,0:T(8,128)(2,1)S(1)}, bf16[384,256]{1,0:T(8,128)(2,1)S(1)}, u32[]{:S(2)}, u32[]{:S(2)}) %collective-permute-start.18) | collective-permute-done | bytes 196640 | tf_op jit(solution)/shard_map/ppermute | solution.py:43
  173.9 1.7 collective-permute-start.19
  176.0 2.7 %hidden_units.7.refs_0_ = bf16[384,256]{1,0:T(8,128)(2,1)S(1)} custom-call(s32[1]{0:T(128)} %bitcast.own_ref, bf16[384,512]{1,0:T(8,128)(2,1)S(1)} %bitcast.31, bf16[384,512]{1,0:T(8,128)(2,1)S(1)} %collective-permute-done.43.refs_1_, bf16[384,512]{1,0:T(8,128)(2,1)S(1)} %collective-permute-done.44.refs_2_, ...), custom_call_target="tpu_custom_call" | custom-call | flops 805306368 | bytes 8388608 | tf_op jit(solution)/shard_map/hidden_units/pallas_call | solution.py:151
  178.7 1.7 collective-permute-start.47
  183.6 2.3 %collective-permute-done.20.refs_3_ = bf16[384,256]{1,0:T(8,128)(2,1)S(1)} collective-permute-done((bf16[384,256]{1,0:T(8,128)(2,1)S(1)}, bf16[384,256]{1,0:T(8,128)(2,1)S(1)}, u32[]{:S(2)}, u32[]{:S(2)}) %collective-permute-start.20) | collective-permute-done | bytes 196640 | tf_op jit(solution)/shard_map/ppermute | solution.py:43
  185.9 1.9 collective-permute-start.46
  187.8 2.3 collective-permute-done.47.refs_2_
  190.1 1.9 collective-permute-start.48
  194.3 1.8 collective-permute-start.21
  196.1 2.3 %collective-permute-done.30.refs_3_ = bf16[384,256]{1,0:T(8,128)(2,1)S(1)} collective-permute-done((bf16[384,256]{1,0:T(8,128)(2,1)S(1)}, bf16[384,256]{1,0:T(8,128)(2,1)S(1)}, u32[]{:S(2)}, u32[]{:S(2)}) %collective-permute-start.30) | collective-permute-done | bytes 196640 | tf_op jit(solution)/shard_map/ppermute | solution.py:43
  200.6 3.4 %collective-permute-start.32 = (bf16[192,512]{1,0:T(8,128)(2,1)S(1)}, bf16[192,512]{1,0:T(8,128)(2,1)S(1)}, u32[]{:S(2)}, u32[]{:S(2)}) collective-permute-start(bf16[192,512]{1,0:T(8,128)(2,1)S(1)} %get-tuple-element.36), channel_id=1, source_target_pairs={{0,20},{4,16},{8,28},{12,24},{16,4},{20,0},{24,12},{28,8},{1,21},{... | collective-permute-start | bytes 589832 | tf_op jit(solution)/shard_map/ppermute | solution.py:36
  207.4 17.9 %collective-permute-done.31.refs_2_ = bf16[192,512]{1,0:T(8,128)(2,1)S(1)} collective-permute-done((bf16[192,512]{1,0:T(8,128)(2,1)S(1)}, bf16[192,512]{1,0:T(8,128)(2,1)S(1)}, u32[]{:S(2)}, u32[]{:S(2)}) %collective-permute-start.31) | collective-permute-done | bytes 196640 | tf_op jit(solution)/shard_map/ppermute | solution.py:36
  225.3 4.2 %collective-permute-done.32.refs_3_ = bf16[192,512]{1,0:T(8,128)(2,1)S(1)} collective-permute-done((bf16[192,512]{1,0:T(8,128)(2,1)S(1)}, bf16[192,512]{1,0:T(8,128)(2,1)S(1)}, u32[]{:S(2)}, u32[]{:S(2)}) %collective-permute-start.32) | collective-permute-done | bytes 196640 | tf_op jit(solution)/shard_map/ppermute | solution.py:36
  (138 shorter events, 40.5 us)
Async XLA Ops:
  2.2 4.5 %collective-permute-start = (bf16[16,2048]{1,0:T(8,128)(2,1)S(1)}, bf16[16,2048]{1,0:T(8,128)(2,1)S(1)}, u32[]{:S(2)}, u32[]{:S(2)}) collective-permute-start(bf16[16,2048]{1,0:T(8,128)(2,1)S(1)} %pad_maximum_fusion.1), channel_id=1, source_target_pairs={{0,4},{4,8},{8,12},{12,16},{16,20},{20,24},{24,28},{1,5},{5,9},{9,... | collective-permute-start | bytes 196616 | tf_op jit(solution)/shard_map/ppermute | solution.py:22
  18.7 8.6 %collective-permute-start.2 = (bf16[144,512]{1,0:T(8,128)(2,1)S(1)}, bf16[144,512]{1,0:T(8,128)(2,1)S(1)}, u32[]{:S(2)}, u32[]{:S(2)}) collective-permute-start(bf16[144,512]{1,0:T(8,128)(2,1)S(1)} %pad_maximum_fusion), channel_id=1, source_target_pairs={{0,8},{4,12},{8,16},{12,20},{16,24},{20,28},{1,9},{5,13},{9,17},{1... | collective-permute-start | bytes 442376 | tf_op jit(solution)/shard_map/ppermute | solution.py:502
  22.2 7.5 %collective-permute-start.4 = (bf16[144,512]{1,0:T(8,128)(2,1)S(1)}, bf16[144,512]{1,0:T(8,128)(2,1)S(1)}, u32[]{:S(2)}, u32[]{:S(2)}) collective-permute-start(bf16[144,512]{1,0:T(8,128)(2,1)S(1)} %pad_maximum_fusion), channel_id=1, source_target_pairs={{0,24},{4,28},{1,25},{5,29},{2,26},{6,30},{3,27},{7,31}} | collective-permute-start | bytes 442376 | tf_op jit(solution)/shard_map/ppermute | solution.py:502
  25.5 6.7 %collective-permute-start.3 = (bf16[144,512]{1,0:T(8,128)(2,1)S(1)}, bf16[144,512]{1,0:T(8,128)(2,1)S(1)}, u32[]{:S(2)}, u32[]{:S(2)}) collective-permute-start(bf16[144,512]{1,0:T(8,128)(2,1)S(1)} %pad_maximum_fusion), channel_id=1, source_target_pairs={{0,16},{4,20},{8,24},{12,28},{1,17},{5,21},{9,25},{13,29},{2,18},{... | collective-permute-start | bytes 442376 | tf_op jit(solution)/shard_map/ppermute | solution.py:502
  32.3 6.1 %collective-permute-start.5 = (bf16[128,512]{1,0:T(8,128)(2,1)S(1)}, bf16[128,512]{1,0:T(8,128)(2,1)S(1)}, u32[]{:S(2)}, u32[]{:S(2)}) collective-permute-start(bf16[128,512]{1,0:T(8,128)(2,1)S(1)} %fusion.6), channel_id=1, source_target_pairs={{0,4},{4,0},{8,12},{12,8},{16,20},{20,16},{24,28},{28,24},{1,5},{5... | collective-permute-start | bytes 393224 | tf_op jit(solution)/shard_map/ppermute | solution.py:31
  45.8 13.0 %collective-permute-start.6 = (bf16[384,512]{1,0:T(8,128)(2,1)S(1)}, bf16[384,512]{1,0:T(8,128)(2,1)S(1)}, u32[]{:S(2)}, u32[]{:S(2)}) collective-permute-start(bf16[384,512]{1,0:T(8,128)(2,1)S(1)} %project_share.5), channel_id=1, source_target_pairs={{0,3},{1,2},{2,1},{3,0},{4,7},{5,6},{6,5},{7,4},{8,11},{9,10},{10,... | collective-permute-start | bytes 1179656 | tf_op jit(solution)/shard_map/ppermute | solution.py:43
  48.4 18.4 %collective-permute-start.7 = (bf16[384,512]{1,0:T(8,128)(2,1)S(1)}, bf16[384,512]{1,0:T(8,128)(2,1)S(1)}, u32[]{:S(2)}, u32[]{:S(2)}) collective-permute-start(bf16[384,512]{1,0:T(8,128)(2,1)S(1)} %project_share.6), channel_id=1, source_target_pairs={{0,2},{1,3},{2,0},{3,1},{4,6},{5,7},{6,4},{7,5},{8,10},{9,11},{10,... | collective-permute-start | bytes 1179656 | tf_op jit(solution)/shard_map/ppermute | solution.py:43
  48.9 17.9 %collective-permute-start.8 = (bf16[384,512]{1,0:T(8,128)(2,1)S(1)}, bf16[384,512]{1,0:T(8,128)(2,1)S(1)}, u32[]{:S(2)}, u32[]{:S(2)}) collective-permute-start(bf16[384,512]{1,0:T(8,128)(2,1)S(1)} %project_share.7), channel_id=1, source_target_pairs={{0,1},{1,0},{2,3},{3,2},{4,5},{5,4},{6,7},{7,6},{8,9},{9,8},{10,11... | collective-permute-start | bytes 1179656 | tf_op jit(solution)/shard_map/ppermute | solution.py:43
  68.1 16.8 %collective-permute-start.9 = (bf16[384,512]{1,0:T(8,128)(2,1)S(1)}, bf16[384,512]{1,0:T(8,128)(2,1)S(1)}, u32[]{:S(2)}, u32[]{:S(2)}) collective-permute-start(bf16[384,512]{1,0:T(8,128)(2,1)S(1)} %get-tuple-element.43.refs_0_), channel_id=1, source_target_pairs={{0,8},{4,12},{8,16},{12,20},{16,24},{20,28},{24,0},{28,4},{1,9},{5... | collective-permute-start | bytes 1179656 | tf_op jit(solution)/shard_map/ppermute | solution.py:36
  84.9 12.2 %collective-permute-start.23 = (bf16[384,512]{1,0:T(8,128)(2,1)S(1)}, bf16[384,512]{1,0:T(8,128)(2,1)S(1)}, u32[]{:S(2)}, u32[]{:S(2)}) collective-permute-start(bf16[384,512]{1,0:T(8,128)(2,1)S(1)} %collective-permute-done.9.refs_0_), channel_id=1, source_target_pairs={{0,8},{4,12},{8,16},{12,20},{16,24},{20,28},{24,0},{28,4},{1,9},{5... | collective-permute-start | bytes 1179656 | tf_op jit(solution)/shard_map/ppermute | solution.py:36
  84.9 27.8 %collective-permute-start.10 = (bf16[384,512]{1,0:T(8,128)(2,1)S(1)}, bf16[384,512]{1,0:T(8,128)(2,1)S(1)}, u32[]{:S(2)}, u32[]{:S(2)}) collective-permute-start(bf16[384,512]{1,0:T(8,128)(2,1)S(1)} %collective-permute-done.9.refs_0_), channel_id=1, source_target_pairs={{0,4},{4,0},{8,12},{12,8},{16,20},{20,16},{24,28},{28,24},{1,5},{5... | collective-permute-start | bytes 1179656 | tf_op jit(solution)/shard_map/ppermute | solution.py:31
  97.0 17.8 %collective-permute-start.41 = (bf16[384,512]{1,0:T(8,128)(2,1)S(1)}, bf16[384,512]{1,0:T(8,128)(2,1)S(1)}, u32[]{:S(2)}, u32[]{:S(2)}) collective-permute-start(bf16[384,512]{1,0:T(8,128)(2,1)S(1)} %collective-permute-done.23.refs_0_), channel_id=1, source_target_pairs={{0,8},{4,12},{8,16},{12,20},{16,24},{20,28},{24,0},{28,4},{1,9},{5... | collective-permute-start | bytes 1179656 | tf_op jit(solution)/shard_map/ppermute | solution.py:36
  97.0 18.0 %collective-permute-start.33 = (bf16[384,512]{1,0:T(8,128)(2,1)S(1)}, bf16[384,512]{1,0:T(8,128)(2,1)S(1)}, u32[]{:S(2)}, u32[]{:S(2)}) collective-permute-start(bf16[384,512]{1,0:T(8,128)(2,1)S(1)} %get-tuple-element.43.refs_0_), channel_id=1, source_target_pairs={{0,4},{4,0},{8,12},{12,8},{16,20},{20,16},{24,28},{28,24},{1,5},{5... | collective-permute-start | bytes 1179656 | tf_op jit(solution)/shard_map/ppermute | solution.py:31
  98.8 9.9 %collective-permute-start.12 = (s32[4,384]{1,0:T(4,128)S(1)}, s32[4,384]{1,0:T(4,128)S(1)}, u32[]{:S(2)}, u32[]{:S(2)}) collective-permute-start(s32[4,384]{1,0:T(4,128)S(1)} %pad_add_fusion), channel_id=1, source_target_pairs={{0,8},{4,12},{8,16},{12,20},{16,24},{20,28},{24,0},{28,4},{1,9},{5... | collective-permute-start | bytes 18440 | tf_op jit(solution)/shard_map/ppermute | solution.py:36
  98.8 9.9 %collective-permute-start.13 = (s32[4,384]{1,0:T(4,128)S(1)}, s32[4,384]{1,0:T(4,128)S(1)}, u32[]{:S(2)}, u32[]{:S(2)}) collective-permute-start(s32[4,384]{1,0:T(4,128)S(1)} %pad_add_fusion), channel_id=1, source_target_pairs={{0,16},{4,20},{8,24},{12,28},{16,0},{20,4},{24,8},{28,12},{1,17},{... | collective-permute-start | bytes 18440 | tf_op jit(solution)/shard_map/ppermute | solution.py:36
  112.6 4.7 %collective-permute-start.24 = (bf16[384,512]{1,0:T(8,128)(2,1)S(1)}, bf16[384,512]{1,0:T(8,128)(2,1)S(1)}, u32[]{:S(2)}, u32[]{:S(2)}) collective-permute-start(bf16[384,512]{1,0:T(8,128)(2,1)S(1)} %collective-permute-done.23.refs_0_), channel_id=1, source_target_pairs={{0,4},{4,0},{8,12},{12,8},{16,20},{20,16},{24,28},{28,24},{1,5},{5... | collective-permute-start | bytes 1179656 | tf_op jit(solution)/shard_map/ppermute | solution.py:31
  113.0 12.1 %collective-permute-start.16 = (bf16[384,512]{1,0:T(8,128)(2,1)S(1)}, bf16[384,512]{1,0:T(8,128)(2,1)S(1)}, u32[]{:S(2)}, u32[]{:S(2)}) collective-permute-start(bf16[384,512]{1,0:T(8,128)(2,1)S(1)} %bitcast.32), channel_id=1, source_target_pairs={{0,2},{1,3},{2,0},{3,1},{4,6},{5,7},{6,4},{7,5},{8,10},{9,11},{10,... | collective-permute-start | bytes 1179656 | tf_op jit(solution)/shard_map/ppermute | solution.py:43
  114.8 11.8 %collective-permute-start.42 = (bf16[384,512]{1,0:T(8,128)(2,1)S(1)}, bf16[384,512]{1,0:T(8,128)(2,1)S(1)}, u32[]{:S(2)}, u32[]{:S(2)}) collective-permute-start(bf16[384,512]{1,0:T(8,128)(2,1)S(1)} %collective-permute-done.41.refs_0_), channel_id=1, source_target_pairs={{0,4},{4,0},{8,12},{12,8},{16,20},{20,16},{24,28},{28,24},{1,5},{5... | collective-permute-start | bytes 1179656 | tf_op jit(solution)/shard_map/ppermute | solution.py:31
  115.4 12.1 %collective-permute-start.34 = (bf16[384,512]{1,0:T(8,128)(2,1)S(1)}, bf16[384,512]{1,0:T(8,128)(2,1)S(1)}, u32[]{:S(2)}, u32[]{:S(2)}) collective-permute-start(bf16[384,512]{1,0:T(8,128)(2,1)S(1)} %bitcast.38), channel_id=1, source_target_pairs={{0,1},{1,0},{2,3},{3,2},{4,5},{5,4},{6,7},{7,6},{8,9},{9,8},{10,11... | collective-permute-start | bytes 1179656 | tf_op jit(solution)/shard_map/ppermute | solution.py:43
  115.6 17.9 %collective-permute-start.35 = (bf16[384,512]{1,0:T(8,128)(2,1)S(1)}, bf16[384,512]{1,0:T(8,128)(2,1)S(1)}, u32[]{:S(2)}, u32[]{:S(2)}) collective-permute-start(bf16[384,512]{1,0:T(8,128)(2,1)S(1)} %bitcast.39), channel_id=1, source_target_pairs={{0,2},{1,3},{2,0},{3,1},{4,6},{5,7},{6,4},{7,5},{8,10},{9,11},{10,... | collective-permute-start | bytes 1179656 | tf_op jit(solution)/shard_map/ppermute | solution.py:43
  117.3 18.6 %collective-permute-start.15 = (bf16[384,512]{1,0:T(8,128)(2,1)S(1)}, bf16[384,512]{1,0:T(8,128)(2,1)S(1)}, u32[]{:S(2)}, u32[]{:S(2)}) collective-permute-start(bf16[384,512]{1,0:T(8,128)(2,1)S(1)} %bitcast.33), channel_id=1, source_target_pairs={{0,1},{1,0},{2,3},{3,2},{4,5},{5,4},{6,7},{7,6},{8,9},{9,8},{10,11... | collective-permute-start | bytes 1179656 | tf_op jit(solution)/shard_map/ppermute | solution.py:43
  125.1 19.2 %collective-permute-start.25 = (bf16[384,512]{1,0:T(8,128)(2,1)S(1)}, bf16[384,512]{1,0:T(8,128)(2,1)S(1)}, u32[]{:S(2)}, u32[]{:S(2)}) collective-permute-start(bf16[384,512]{1,0:T(8,128)(2,1)S(1)} %bitcast.35), channel_id=1, source_target_pairs={{0,1},{1,0},{2,3},{3,2},{4,5},{5,4},{6,7},{7,6},{8,9},{9,8},{10,11... | collective-permute-start | bytes 1179656 | tf_op jit(solution)/shard_map/ppermute | solution.py:43
  126.6 26.1 %collective-permute-start.17 = (bf16[384,512]{1,0:T(8,128)(2,1)S(1)}, bf16[384,512]{1,0:T(8,128)(2,1)S(1)}, u32[]{:S(2)}, u32[]{:S(2)}) collective-permute-start(bf16[384,512]{1,0:T(8,128)(2,1)S(1)} %collective-permute-done.16.refs_2_), channel_id=1, source_target_pairs={{0,1},{1,0},{2,3},{3,2},{4,5},{5,4},{6,7},{7,6},{8,9},{9,8},{10,11... | collective-permute-start | bytes 1179656 | tf_op jit(solution)/shard_map/ppermute | solution.py:43
  127.5 25.6 %collective-permute-start.44 = (bf16[384,512]{1,0:T(8,128)(2,1)S(1)}, bf16[384,512]{1,0:T(8,128)(2,1)S(1)}, u32[]{:S(2)}, u32[]{:S(2)}) collective-permute-start(bf16[384,512]{1,0:T(8,128)(2,1)S(1)} %bitcast.29), channel_id=1, source_target_pairs={{0,2},{1,3},{2,0},{3,1},{4,6},{5,7},{6,4},{7,5},{8,10},{9,11},{10,... | collective-permute-start | bytes 1179656 | tf_op jit(solution)/shard_map/ppermute | solution.py:43
  133.5 26.3 %collective-permute-start.36 = (bf16[384,512]{1,0:T(8,128)(2,1)S(1)}, bf16[384,512]{1,0:T(8,128)(2,1)S(1)}, u32[]{:S(2)}, u32[]{:S(2)}) collective-permute-start(bf16[384,512]{1,0:T(8,128)(2,1)S(1)} %collective-permute-done.34.refs_1_), channel_id=1, source_target_pairs={{0,2},{1,3},{2,0},{3,1},{4,6},{5,7},{6,4},{7,5},{8,10},{9,11},{10,... | collective-permute-start | bytes 1179656 | tf_op jit(solution)/shard_map/ppermute | solution.py:43
  135.9 27.4 %collective-permute-start.26 = (bf16[384,512]{1,0:T(8,128)(2,1)S(1)}, bf16[384,512]{1,0:T(8,128)(2,1)S(1)}, u32[]{:S(2)}, u32[]{:S(2)}) collective-permute-start(bf16[384,512]{1,0:T(8,128)(2,1)S(1)} %bitcast.36), channel_id=1, source_target_pairs={{0,2},{1,3},{2,0},{3,1},{4,6},{5,7},{6,4},{7,5},{8,10},{9,11},{10,... | collective-permute-start | bytes 1179656 | tf_op jit(solution)/shard_map/ppermute | solution.py:43
  144.3 29.6 %collective-permute-start.43 = (bf16[384,512]{1,0:T(8,128)(2,1)S(1)}, bf16[384,512]{1,0:T(8,128)(2,1)S(1)}, u32[]{:S(2)}, u32[]{:S(2)}) collective-permute-start(bf16[384,512]{1,0:T(8,128)(2,1)S(1)} %bitcast.30), channel_id=1, source_target_pairs={{0,1},{1,0},{2,3},{3,2},{4,5},{5,4},{6,7},{7,6},{8,9},{9,8},{10,11... | collective-permute-start | bytes 1179656 | tf_op jit(solution)/shard_map/ppermute | solution.py:43
  152.7 14.0 %collective-permute-start.27 = (bf16[384,512]{1,0:T(8,128)(2,1)S(1)}, bf16[384,512]{1,0:T(8,128)(2,1)S(1)}, u32[]{:S(2)}, u32[]{:S(2)}) collective-permute-start(bf16[384,512]{1,0:T(8,128)(2,1)S(1)} %collective-permute-done.25.refs_1_), channel_id=1, source_target_pairs={{0,2},{1,3},{2,0},{3,1},{4,6},{5,7},{6,4},{7,5},{8,10},{9,11},{10,... | collective-permute-start | bytes 1179656 | tf_op jit(solution)/shard_map/ppermute | solution.py:43
  153.1 22.5 %collective-permute-start.45 = (bf16[384,512]{1,0:T(8,128)(2,1)S(1)}, bf16[384,512]{1,0:T(8,128)(2,1)S(1)}, u32[]{:S(2)}, u32[]{:S(2)}) collective-permute-start(bf16[384,512]{1,0:T(8,128)(2,1)S(1)} %collective-permute-done.44.refs_2_), channel_id=1, source_target_pairs={{0,1},{1,0},{2,3},{3,2},{4,5},{5,4},{6,7},{7,6},{8,9},{9,8},{10,11... | collective-permute-start | bytes 1179656 | tf_op jit(solution)/shard_map/ppermute | solution.py:43
  159.8 14.0 %collective-permute-start.18 = (bf16[384,256]{1,0:T(8,128)(2,1)S(1)}, bf16[384,256]{1,0:T(8,128)(2,1)S(1)}, u32[]{:S(2)}, u32[]{:S(2)}) collective-permute-start(bf16[384,256]{1,0:T(8,128)(2,1)S(1)} %hidden_units.4.refs_0_), channel_id=1, source_target_pairs={{0,1},{1,0},{2,3},{3,2},{4,5},{5,4},{6,7},{7,6},{8,9},{9,8},{10,11... | collective-permute-start | bytes 589832 | tf_op jit(solution)/shard_map/ppermute | solution.py:43
  163.3 15.5 %collective-permute-start.37 = (bf16[384,256]{1,0:T(8,128)(2,1)S(1)}, bf16[384,256]{1,0:T(8,128)(2,1)S(1)}, u32[]{:S(2)}, u32[]{:S(2)}) collective-permute-start(bf16[384,256]{1,0:T(8,128)(2,1)S(1)} %hidden_units.6.refs_0_), channel_id=1, source_target_pairs={{0,1},{1,0},{2,3},{3,2},{4,5},{5,4},{6,7},{7,6},{8,9},{9,8},{10,11... | collective-permute-start | bytes 589832 | tf_op jit(solution)/shard_map/ppermute | solution.py:43
  166.7 13.7 %collective-permute-start.38 = (bf16[384,256]{1,0:T(8,128)(2,1)S(1)}, bf16[384,256]{1,0:T(8,128)(2,1)S(1)}, u32[]{:S(2)}, u32[]{:S(2)}) collective-permute-start(bf16[384,256]{1,0:T(8,128)(2,1)S(1)} %hidden_units.6.refs_0_), channel_id=1, source_target_pairs={{0,2},{1,3},{2,0},{3,1},{4,6},{5,7},{6,4},{7,5},{8,10},{9,11},{10,... | collective-permute-start | bytes 589832 | tf_op jit(solution)/shard_map/ppermute | solution.py:43
  173.8 7.8 %collective-permute-start.28 = (bf16[384,256]{1,0:T(8,128)(2,1)S(1)}, bf16[384,256]{1,0:T(8,128)(2,1)S(1)}, u32[]{:S(2)}, u32[]{:S(2)}) collective-permute-start(bf16[384,256]{1,0:T(8,128)(2,1)S(1)} %hidden_units.5.refs_0_), channel_id=1, source_target_pairs={{0,1},{1,0},{2,3},{3,2},{4,5},{5,4},{6,7},{7,6},{8,9},{9,8},{10,11... | collective-permute-start | bytes 589832 | tf_op jit(solution)/shard_map/ppermute | solution.py:43
  173.9 8.6 %collective-permute-start.19 = (bf16[384,256]{1,0:T(8,128)(2,1)S(1)}, bf16[384,256]{1,0:T(8,128)(2,1)S(1)}, u32[]{:S(2)}, u32[]{:S(2)}) collective-permute-start(bf16[384,256]{1,0:T(8,128)(2,1)S(1)} %hidden_units.4.refs_0_), channel_id=1, source_target_pairs={{0,2},{1,3},{2,0},{3,1},{4,6},{5,7},{6,4},{7,5},{8,10},{9,11},{10,... | collective-permute-start | bytes 589832 | tf_op jit(solution)/shard_map/ppermute | solution.py:43
  175.6 10.3 %collective-permute-start.20 = (bf16[384,256]{1,0:T(8,128)(2,1)S(1)}, bf16[384,256]{1,0:T(8,128)(2,1)S(1)}, u32[]{:S(2)}, u32[]{:S(2)}) collective-permute-start(bf16[384,256]{1,0:T(8,128)(2,1)S(1)} %collective-permute-done.18.refs_1_), channel_id=1, source_target_pairs={{0,2},{1,3},{2,0},{3,1},{4,6},{5,7},{6,4},{7,5},{8,10},{9,11},{10,... | collective-permute-start | bytes 589832 | tf_op jit(solution)/shard_map/ppermute | solution.py:43
  178.7 11.4 %collective-permute-start.47 = (bf16[384,256]{1,0:T(8,128)(2,1)S(1)}, bf16[384,256]{1,0:T(8,128)(2,1)S(1)}, u32[]{:S(2)}, u32[]{:S(2)}) collective-permute-start(bf16[384,256]{1,0:T(8,128)(2,1)S(1)} %hidden_units.7.refs_0_), channel_id=1, source_target_pairs={{0,2},{1,3},{2,0},{3,1},{4,6},{5,7},{6,4},{7,5},{8,10},{9,11},{10,... | collective-permute-start | bytes 589832 | tf_op jit(solution)/shard_map/ppermute | solution.py:43
  180.4 13.9 %collective-permute-start.29 = (bf16[384,256]{1,0:T(8,128)(2,1)S(1)}, bf16[384,256]{1,0:T(8,128)(2,1)S(1)}, u32[]{:S(2)}, u32[]{:S(2)}) collective-permute-start(bf16[384,256]{1,0:T(8,128)(2,1)S(1)} %hidden_units.5.refs_0_), channel_id=1, source_target_pairs={{0,2},{1,3},{2,0},{3,1},{4,6},{5,7},{6,4},{7,5},{8,10},{9,11},{10,... | collective-permute-start | bytes 589832 | tf_op jit(solution)/shard_map/ppermute | solution.py:43
  181.5 16.9 %collective-permute-start.30 = (bf16[384,256]{1,0:T(8,128)(2,1)S(1)}, bf16[384,256]{1,0:T(8,128)(2,1)S(1)}, u32[]{:S(2)}, u32[]{:S(2)}) collective-permute-start(bf16[384,256]{1,0:T(8,128)(2,1)S(1)} %collective-permute-done.28.refs_1_), channel_id=1, source_target_pairs={{0,2},{1,3},{2,0},{3,1},{4,6},{5,7},{6,4},{7,5},{8,10},{9,11},{10,... | collective-permute-start | bytes 589832 | tf_op jit(solution)/shard_map/ppermute | solution.py:43
  182.5 18.1 %collective-permute-start.39 = (bf16[384,256]{1,0:T(8,128)(2,1)S(1)}, bf16[384,256]{1,0:T(8,128)(2,1)S(1)}, u32[]{:S(2)}, u32[]{:S(2)}) collective-permute-start(bf16[384,256]{1,0:T(8,128)(2,1)S(1)} %collective-permute-done.37.refs_1_), channel_id=1, source_target_pairs={{0,2},{1,3},{2,0},{3,1},{4,6},{5,7},{6,4},{7,5},{8,10},{9,11},{10,... | collective-permute-start | bytes 589832 | tf_op jit(solution)/shard_map/ppermute | solution.py:43
  185.9 14.7 %collective-permute-start.46 = (bf16[384,256]{1,0:T(8,128)(2,1)S(1)}, bf16[384,256]{1,0:T(8,128)(2,1)S(1)}, u32[]{:S(2)}, u32[]{:S(2)}) collective-permute-start(bf16[384,256]{1,0:T(8,128)(2,1)S(1)} %hidden_units.7.refs_0_), channel_id=1, source_target_pairs={{0,1},{1,0},{2,3},{3,2},{4,5},{5,4},{6,7},{7,6},{8,9},{9,8},{10,11... | collective-permute-start | bytes 589832 | tf_op jit(solution)/shard_map/ppermute | solution.py:43
  190.1 15.1 %collective-permute-start.48 = (bf16[384,256]{1,0:T(8,128)(2,1)S(1)}, bf16[384,256]{1,0:T(8,128)(2,1)S(1)}, u32[]{:S(2)}, u32[]{:S(2)}) collective-permute-start(bf16[384,256]{1,0:T(8,128)(2,1)S(1)} %collective-permute-done.47.refs_2_), channel_id=1, source_target_pairs={{0,1},{1,0},{2,3},{3,2},{4,5},{5,4},{6,7},{7,6},{8,9},{9,8},{10,11... | collective-permute-start | bytes 589832 | tf_op jit(solution)/shard_map/ppermute | solution.py:43
  194.3 12.2 %collective-permute-start.21 = (bf16[192,512]{1,0:T(8,128)(2,1)S(1)}, bf16[192,512]{1,0:T(8,128)(2,1)S(1)}, u32[]{:S(2)}, u32[]{:S(2)}) collective-permute-start(bf16[192,512]{1,0:T(8,128)(2,1)S(1)} %get-tuple-element.33), channel_id=1, source_target_pairs={{0,24},{4,28},{8,0},{12,4},{16,8},{20,12},{24,16},{28,20},{1,25},{... | collective-permute-start | bytes 589832 | tf_op jit(solution)/shard_map/ppermute | solution.py:36
  198.5 8.4 %collective-permute-start.22 = (bf16[192,512]{1,0:T(8,128)(2,1)S(1)}, bf16[192,512]{1,0:T(8,128)(2,1)S(1)}, u32[]{:S(2)}, u32[]{:S(2)}) collective-permute-start(bf16[192,512]{1,0:T(8,128)(2,1)S(1)} %get-tuple-element.34), channel_id=1, source_target_pairs={{0,28},{4,24},{8,4},{12,0},{16,12},{20,8},{24,20},{28,16},{1,29},{... | collective-permute-start | bytes 589832 | tf_op jit(solution)/shard_map/ppermute | solution.py:36
  200.6 24.7 %collective-permute-start.31 = (bf16[192,512]{1,0:T(8,128)(2,1)S(1)}, bf16[192,512]{1,0:T(8,128)(2,1)S(1)}, u32[]{:S(2)}, u32[]{:S(2)}) collective-permute-start(bf16[192,512]{1,0:T(8,128)(2,1)S(1)} %get-tuple-element.35), channel_id=1, source_target_pairs={{0,16},{4,20},{8,24},{12,28},{16,0},{20,4},{24,8},{28,12},{1,17},{... | collective-permute-start | bytes 589832 | tf_op jit(solution)/shard_map/ppermute | solution.py:36
  200.6 28.9 %collective-permute-start.32 = (bf16[192,512]{1,0:T(8,128)(2,1)S(1)}, bf16[192,512]{1,0:T(8,128)(2,1)S(1)}, u32[]{:S(2)}, u32[]{:S(2)}) collective-permute-start(bf16[192,512]{1,0:T(8,128)(2,1)S(1)} %get-tuple-element.36), channel_id=1, source_target_pairs={{0,20},{4,16},{8,28},{12,24},{16,4},{20,0},{24,12},{28,8},{1,21},{... | collective-permute-start | bytes 589832 | tf_op jit(solution)/shard_map/ppermute | solution.py:36
  205.2 25.3 %collective-permute-start.40 = (bf16[192,512]{1,0:T(8,128)(2,1)S(1)}, bf16[192,512]{1,0:T(8,128)(2,1)S(1)}, u32[]{:S(2)}, u32[]{:S(2)}) collective-permute-start(bf16[192,512]{1,0:T(8,128)(2,1)S(1)} %get-tuple-element.40), channel_id=1, source_target_pairs={{0,4},{4,0},{8,12},{12,8},{16,20},{20,16},{24,28},{28,24},{1,5},{5... | collective-permute-start | bytes 589832 | tf_op jit(solution)/shard_map/ppermute | solution.py:36
  206.6 24.6 %collective-permute-start.49 = (bf16[192,512]{1,0:T(8,128)(2,1)S(1)}, bf16[192,512]{1,0:T(8,128)(2,1)S(1)}, u32[]{:S(2)}, u32[]{:S(2)}) collective-permute-start(bf16[192,512]{1,0:T(8,128)(2,1)S(1)} %get-tuple-element.41), channel_id=1, source_target_pairs={{0,8},{4,12},{8,16},{12,20},{16,24},{20,28},{24,0},{28,4},{1,9},{5... | collective-permute-start | bytes 589832 | tf_op jit(solution)/shard_map/ppermute | solution.py:36
  206.9 24.3 %collective-permute-start.50 = (bf16[192,512]{1,0:T(8,128)(2,1)S(1)}, bf16[192,512]{1,0:T(8,128)(2,1)S(1)}, u32[]{:S(2)}, u32[]{:S(2)}) collective-permute-start(bf16[192,512]{1,0:T(8,128)(2,1)S(1)} %get-tuple-element.42), channel_id=1, source_target_pairs={{0,12},{4,8},{8,20},{12,16},{16,28},{20,24},{24,4},{28,0},{1,13},{... | collective-permute-start | bytes 589832 | tf_op jit(solution)/shard_map/ppermute | solution.py:36
  (19 other events, 229.4 us)
